TPU v7x, 32 devices: a whole 2x2x4 slice. The times are simulated.
32 devices in a mesh: grp: 2 (over y), sp: 4 (over z), fs: 2 (over x), tp: 2 (over core).
Axes of the slice: x: 2, y: 2, z: 4, core: 2. Of those that a mesh axis runs over, the one named last changes fastest.
Arguments:
- tokens: bfloat16 [8, 512, 2048], P(('grp', 'fs'), ('sp', 'tp')), parts along dimension 0, may hold values from -24 to 24
- norm_gain: float32 [2048], replicated, may hold values from 0.1 to 1.9
- w_query: bfloat16 [2048, 1024], P(('sp', 'fs'), 'tp'), may hold values from -0.125 to 0.125
- w_key: bfloat16 [2048, 1024], P(('sp', 'fs'), 'tp'), may hold values from -0.125 to 0.125
- w_value: bfloat16 [2048, 1024], P(('sp', 'fs'), 'tp'), may hold values from -0.125 to 0.125
- query_gain: float32 [1024], P('tp'), may hold values from 1 to 26
- key_gain: float32 [1024], P('tp'), may hold values from 0.1 to 1.9
- mix_lambda: float32 [8], P('tp'), may hold values from 0.3 to 0.8
- head_gain: float32 [128], replicated, may hold values from 0.1 to 1.9
- w_gate_b: bfloat16 [2048, 1024], P(('sp', 'fs'), 'tp'), may hold values from -0.125 to 0.125
- w_gate_c: bfloat16 [2048, 1024], P(('sp', 'fs'), 'tp'), may hold values from -0.125 to 0.125
- w_conv_in: bfloat16 [2048, 1024], P(('sp', 'fs'), 'tp'), may hold values from -0.125 to 0.125
- conv_taps: float32 [3, 1024], P(None, 'tp'), may hold values from -3 to 3
- w_out_attn: bfloat16 [1024, 2048], P('tp', ('sp', 'fs')), may hold values from -0.125 to 0.125
- w_out_conv: bfloat16 [1024, 2048], P('tp', ('sp', 'fs')), may hold values from -0.125 to 0.125
Outputs:
- mixed: bfloat16 [8, 512, 2048], P(('grp', 'fs'), ('sp', 'tp')), parts along dimension 0
There are 2 independent parts, one for each index of `grp`. A program takes and returns all parts, laid end to end along the dimension named above; an argument that names none is the same for every part. Nothing has to cross between parts.
All inputs are finite; a program needn't handle non-finite values.
Results may differ from a plain program's by a relative error of at most 0.04.
Values may be sent and summed in bfloat16 or wider, within the bound.
A program may use at most 128 MiB of HBM per device.

v0:
```python
import math

import jax
import jax.numpy as jnp
from jax import lax
from jax.sharding import PartitionSpec as P

DK = 64
DV = 128
KW = 3


EPS = 1e-06
NEG = -1e30
OUT_SCALE = 0.8


def from_behind(block, axis, distance):
    devices = range(lax.axis_size(axis))
    route = [(i - distance, i) for i in devices if i - distance in devices]
    return lax.ppermute(block, axis, route)


def rms_scale(values, gain):
    wide = values.astype(jnp.float32)
    return wide * lax.rsqrt(jnp.mean(wide * wide, axis=-1, keepdims=True) + EPS) * gain


def attend_heads(normed, wq_full, wk_full, wv_full, query_gain, key_gain, mix_lambda, head_gain):
    rows = normed.shape[0]
    heads_here = mix_lambda.shape[0]
    query = rms_scale(
        jnp.dot(normed, wq_full, preferred_element_type=jnp.float32)
        .astype(jnp.bfloat16)
        .reshape(rows, heads_here, 2, DK),
        query_gain.reshape(heads_here, 2, DK),
    ).astype(jnp.bfloat16)
    key = rms_scale(
        jnp.dot(normed, wk_full, preferred_element_type=jnp.float32)
        .astype(jnp.bfloat16)
        .reshape(rows, heads_here, 2, DK),
        key_gain.reshape(heads_here, 2, DK),
    ).astype(jnp.bfloat16)
    value = jnp.dot(normed, wv_full, preferred_element_type=jnp.float32).astype(jnp.bfloat16)
    q_pos = lax.axis_index("sp") * rows + jnp.arange(rows, dtype=jnp.int32)
    init = (
        jnp.full((heads_here, 2, rows), NEG, jnp.float32),
        jnp.zeros((heads_here, 2, rows), jnp.float32),
        jnp.zeros((heads_here, 2, rows, DV), jnp.float32),
    )
    key_piece = lax.all_gather(key.reshape(rows, heads_here * 2 * DK), "sp", axis=0, tiled=True)
    value_piece = lax.all_gather(value, "sp", axis=0, tiled=True)
    count = key_piece.shape[0]
    width = math.gcd(count, 1024)
    blocks = count // width
    key_blocks = key_piece.reshape(blocks, width, heads_here, 2, DK)
    value_blocks = value_piece.reshape(blocks, width, heads_here, DV)
    begins = jnp.arange(blocks, dtype=jnp.int32) * width

    def step(state, inputs):
        running, total, summed = state
        key_block, value_block, begin = inputs
        k_pos = begin + jnp.arange(width, dtype=jnp.int32)
        score = jnp.einsum(
            "qhmd,khmd->hmqk", query, key_block, preferred_element_type=jnp.float32
        ) * DK ** (-0.5)
        allowed = k_pos[None, :] <= q_pos[:, None]
        score = jnp.where(allowed, score, NEG)
        newest = jnp.maximum(running, jnp.max(score, axis=-1))
        factor = jnp.exp(running - newest)
        weights = jnp.where(allowed, jnp.exp(score - newest[..., None]), 0.0)
        total = total * factor + jnp.sum(weights, axis=-1)
        summed = summed * factor[..., None] + jnp.einsum(
            "hmqk,khd->hmqd",
            weights.astype(jnp.bfloat16),
            value_block,
            preferred_element_type=jnp.float32,
        )
        return ((newest, total, summed), None)

    result, unused = lax.scan(step, init, (key_blocks, value_blocks, begins))
    running, total, summed = result
    head_map = summed / total[..., None]
    differ = head_map[:, 0] - mix_lambda[:, None, None] * head_map[:, 1]
    normal = rms_scale(differ, head_gain) * OUT_SCALE
    return normal.transpose(1, 0, 2).reshape(rows, heads_here * DV).astype(jnp.bfloat16)


def gated_conv(normed, wb_full, wc_full, wi_full, conv_taps):
    rows = normed.shape[0]
    gate_b = jnp.dot(normed, wb_full, preferred_element_type=jnp.float32).astype(jnp.bfloat16)
    gate_c = jnp.dot(normed, wc_full, preferred_element_type=jnp.float32).astype(jnp.bfloat16)
    conv_in = jnp.dot(normed, wi_full, preferred_element_type=jnp.float32).astype(jnp.bfloat16)
    shaped = (gate_c.astype(jnp.float32) * conv_in.astype(jnp.float32)).astype(jnp.bfloat16)
    edge = from_behind(shaped[rows - (KW - 1) :], "sp", 1)
    padded = jnp.concatenate([edge, shaped], axis=0).astype(jnp.float32)
    conv = conv_taps[0][None, :] * padded[0:rows]
    for tap in range(1, KW):
        conv = conv + conv_taps[tap][None, :] * padded[tap : tap + rows]
    return (gate_b.astype(jnp.float32) * conv).astype(jnp.bfloat16)


def normalize_rows(own_rows, norm_gain):
    return rms_scale(lax.all_gather(own_rows, "tp", axis=0, tiled=True), norm_gain).astype(
        jnp.bfloat16
    )


def on_device(
    tokens,
    norm_gain,
    w_query,
    w_key,
    w_value,
    query_gain,
    key_gain,
    mix_lambda,
    head_gain,
    w_gate_b,
    w_gate_c,
    w_conv_in,
    conv_taps,
    w_out_attn,
    w_out_conv,
):
    seq_count = tokens.shape[0]
    gathered = (
        lax.all_gather(w_query, ("sp", "fs"), axis=0, tiled=True),
        lax.all_gather(w_key, ("sp", "fs"), axis=0, tiled=True),
        lax.all_gather(w_value, ("sp", "fs"), axis=0, tiled=True),
        lax.all_gather(w_gate_b, ("sp", "fs"), axis=0, tiled=True),
        lax.all_gather(w_gate_c, ("sp", "fs"), axis=0, tiled=True),
        lax.all_gather(w_conv_in, ("sp", "fs"), axis=0, tiled=True),
        lax.all_gather(w_out_attn, ("sp", "fs"), axis=1, tiled=True),
        lax.all_gather(w_out_conv, ("sp", "fs"), axis=1, tiled=True),
    )
    normed_list = [normalize_rows(tokens[index], norm_gain) for index in range(seq_count)]
    attn_list = [
        attend_heads(
            normed,
            gathered[0],
            gathered[1],
            gathered[2],
            query_gain,
            key_gain,
            mix_lambda,
            head_gain,
        )
        for normed in normed_list
    ]
    conv_list = [
        gated_conv(normed, gathered[3], gathered[4], gathered[5], conv_taps)
        for normed in normed_list
    ]
    out_attn = gathered[6]
    out_conv = gathered[7]
    results = []
    for index in range(seq_count):
        attn = attn_list[index]
        conv_out = conv_list[index]
        results.append(
            lax.psum_scatter(
                (
                    jnp.dot(attn, out_attn, preferred_element_type=jnp.float32)
                    + jnp.dot(conv_out, out_conv, preferred_element_type=jnp.float32)
                ).astype(jnp.bfloat16),
                "tp",
                scatter_dimension=0,
                tiled=True,
            )
        )
    return jnp.stack(results, axis=0)


def solution(mesh):
    placed = (
        P(("grp", "fs"), ("sp", "tp"), None),
        P(),
        P(("sp", "fs"), "tp"),
        P(("sp", "fs"), "tp"),
        P(("sp", "fs"), "tp"),
        P("tp"),
        P("tp"),
        P("tp"),
        P(),
        P(("sp", "fs"), "tp"),
        P(("sp", "fs"), "tp"),
        P(("sp", "fs"), "tp"),
        P(None, "tp"),
        P("tp", ("sp", "fs")),
        P("tp", ("sp", "fs")),
    )
    return jax.shard_map(
        on_device,
        mesh=mesh,
        in_specs=placed,
        out_specs=P(("grp", "fs"), ("sp", "tp"), None),
        check_vma=False,
    )
```

profile of v0, /device:TPU:0, one launch (start us, length us, event | category | flops | bytes accessed | tf_op | source)
XLA Modules:
  0.0 453.7 jit_solution(17097135816359609861)
XLA Ops:
  12.1 2.3 all-gather
  14.6 2.2 all-gather.1
  17.2 44.2 %all-gather.13.cloned.1.call-done = bf16[2048,512]{1,0:T(8,128)(2,1)} async-done(((bf16[256,512]{1,0:T(8,128)(2,1)}), bf16[2048,512]{1,0:T(8,128)(2,1)}) %all-gather.13.cloned.1.call-update) | async-done | bytes 2097168 | tf_op jit(solution)/shard_map/all_gather | solution.py:129
  61.4 3.0 fusion.86
  71.8 20.0 %all_gather.45 = bf16[512,512]{1,0:T(8,128)(2,1)S(1)} all-gather(bf16[128,512]{1,0:T(8,128)(2,1)S(1)} %get-tuple-element.69), channel_id=1, replica_groups=mesh['grp'=2,'sp'=4,'fs'=2,'tp'=2] {'sp'}, dimensions={0}, use_global_device_ids=true | all-gather | bytes 655360 | tf_op jit(solution)/shard_map/all_gather | solution.py:51
  92.8 24.1 %all-gather.11.cloned.1.call-done = bf16[2048,512]{1,0:T(8,128)(2,1)} async-done(((bf16[256,512]{1,0:T(8,128)(2,1)}), bf16[2048,512]{1,0:T(8,128)(2,1)}) %all-gather.11.cloned.1.call-update) | async-done | bytes 2097168 | tf_op jit(solution)/shard_map/all_gather | solution.py:128
  119.2 3.2 fusion.2
  122.4 20.8 %all_gather.54 = bf16[512,512]{1,0:T(8,128)(2,1)} all-gather(bf16[128,512]{1,0:T(8,128)(2,1)S(1)} %copy-done.11), channel_id=1, replica_groups=mesh['grp'=2,'sp'=4,'fs'=2,'tp'=2] {'sp'}, dimensions={0}, use_global_device_ids=true | all-gather | bytes 655360 | tf_op jit(solution)/shard_map/all_gather | solution.py:51
  145.9 3.0 fusion.4
  149.7 20.3 %all-gather.15.cloned.1.call-done = bf16[2048,512]{1,0:T(8,128)(2,1)} async-done(((bf16[256,512]{1,0:T(8,128)(2,1)}), bf16[2048,512]{1,0:T(8,128)(2,1)}) %all-gather.15.cloned.1.call-update) | async-done | bytes 2097168 | tf_op jit(solution)/shard_map/all_gather | solution.py:130
  170.0 2.1 convolution_convert_fusion.3
  172.1 19.2 %all_gather.55 = bf16[512,512]{1,0:T(8,128)(2,1)S(1)} all-gather(bf16[128,512]{1,0:T(8,128)(2,1)S(1)} %convolution_convert_fusion.3), channel_id=1, replica_groups=mesh['grp'=2,'sp'=4,'fs'=2,'tp'=2] {'sp'}, dimensions={0}, use_global_device_ids=true | all-gather | bytes 655360 | tf_op jit(solution)/shard_map/all_gather | solution.py:52
  191.5 2.1 convolution_convert_fusion.9
  193.6 18.4 %all_gather.47 = bf16[512,512]{1,0:T(8,128)(2,1)S(1)} all-gather(bf16[128,512]{1,0:T(8,128)(2,1)S(1)} %convolution_convert_fusion.9), channel_id=1, replica_groups=mesh['grp'=2,'sp'=4,'fs'=2,'tp'=2] {'sp'}, dimensions={0}, use_global_device_ids=true | all-gather | bytes 655360 | tf_op jit(solution)/shard_map/all_gather | solution.py:52
  213.0 8.9 %all-gather.21.cloned.1.call-done = bf16[2048,512]{1,0:T(8,128)(2,1)} async-done(((bf16[256,512]{1,0:T(8,128)(2,1)}), bf16[2048,512]{1,0:T(8,128)(2,1)}) %all-gather.21.cloned.1.call-update) | async-done | bytes 2097168 | tf_op jit(solution)/shard_map/all_gather | solution.py:132
  224.0 48.0 %all-gather.23.cloned.1.call-done = bf16[2048,512]{1,0:T(8,128)(2,1)} async-done(((bf16[256,512]{1,0:T(8,128)(2,1)}), bf16[2048,512]{1,0:T(8,128)(2,1)}) %all-gather.23.cloned.1.call-update) | async-done | bytes 2097168 | tf_op jit(solution)/shard_map/all_gather | solution.py:133
  274.1 3.7 collective-permute-start
  280.2 42.6 %all-gather.17.cloned.1.call-done = bf16[512,2048]{1,0:T(8,128)(2,1)} async-done(((bf16[512,256]{1,0:T(8,128)(2,1)}), bf16[512,2048]{1,0:T(8,128)(2,1)}) %all-gather.17.cloned.1.call-update) | async-done | bytes 2097168 | tf_op jit(solution)/shard_map/all_gather | solution.py:134
  322.8 3.0 fusion.87
  327.1 45.1 %all-gather.19.cloned.1.call-done = bf16[2048,512]{1,0:T(8,128)(2,1)} async-done(((bf16[256,512]{1,0:T(8,128)(2,1)}), bf16[2048,512]{1,0:T(8,128)(2,1)}) %all-gather.19.cloned.1.call-update) | async-done | bytes 2097168 | tf_op jit(solution)/shard_map/all_gather | solution.py:131
  372.2 51.0 %all-gather.25.cloned.1.call-done = bf16[512,2048]{1,0:T(8,128)(2,1)} async-done(((bf16[512,256]{1,0:T(8,128)(2,1)}), bf16[512,2048]{1,0:T(8,128)(2,1)}) %all-gather.25.cloned.1.call-update) | async-done | bytes 2097168 | tf_op jit(solution)/shard_map/all_gather | solution.py:135
  423.2 4.4 fusion
  432.5 3.6 fusion.1
  436.2 8.8 %reduce-scatter.5.cloned.1.call-done = bf16[64,2048]{1,0:T(8,128)(2,1)} async-done(((bf16[128,2048]{1,0:T(8,128)(2,1)}), bf16[64,2048]{1,0:T(8,128)(2,1)}) %reduce-scatter.5.cloned.1.call-update) | async-done | bytes 262160 | tf_op jit(solution)/shard_map/reduce_scatter | solution.py:162
  (117 shorter events, 35.7 us)
Async XLA Ops:
  6.5 5.5 %copy-start.12 = (bf16[2,64,2048]{2,1,0:T(8,128)(2,1)S(1)}, bf16[2,64,2048]{2,1,0:T(8,128)(2,1)}, u32[]{:S(2)}) copy-start(bf16[2,64,2048]{2,1,0:T(8,128)(2,1)} %param.15) | copy-start | bytes 1572868
  6.5 54.8 %all-gather.13.cloned.1.call-start = ((), (), s32[]{:S(2)}) async-start(), calls=%async_computation.3 | async-start | bytes 2359296 | tf_op jit(solution)/shard_map/all_gather | solution.py:129
  7.3 109.6 %all-gather.11.cloned.1.call-start = ((), (), s32[]{:S(2)}) async-start(), calls=%async_computation.2 | async-start | bytes 2359296 | tf_op jit(solution)/shard_map/all_gather | solution.py:128
  8.0 162.0 %all-gather.15.cloned.1.call-start = ((), (), s32[]{:S(2)}) async-start(), calls=%async_computation.4 | async-start | bytes 2359296 | tf_op jit(solution)/shard_map/all_gather | solution.py:130
  8.7 213.2 %all-gather.21.cloned.1.call-start = ((), (), s32[]{:S(2)}) async-start(), calls=%async_computation.7 | async-start | bytes 2359296 | tf_op jit(solution)/shard_map/all_gather | solution.py:132
  9.3 262.7 %all-gather.23.cloned.1.call-start = ((), (), s32[]{:S(2)}) async-start(), calls=%async_computation.8 | async-start | bytes 2359296 | tf_op jit(solution)/shard_map/all_gather | solution.py:133
  9.9 312.9 %all-gather.17.cloned.1.call-start = ((), (), s32[]{:S(2)}) async-start(), calls=%async_computation.5 | async-start | bytes 2359296 | tf_op jit(solution)/shard_map/all_gather | solution.py:134
  10.5 6.6 %copy-start.17 = (f32[512]{0:T(512)S(1)}, f32[512]{0:T(512)}, u32[]{:S(2)}) copy-start(f32[512]{0:T(512)} %param.20) | copy-start | bytes 6148
  10.5 6.7 %copy-start.14 = (f32[3,512]{1,0:T(4,128)S(1)}, f32[3,512]{1,0:T(4,128)}, u32[]{:S(2)}) copy-start(f32[3,512]{1,0:T(4,128)} %param.27) | copy-start | bytes 18436
  10.5 50.9 %copy-start.7 = (f32[2048]{0:T(1024)S(1)}, f32[2048]{0:T(1024)}, u32[]{:S(2)}) copy-start(f32[2048]{0:T(1024)} %param.16) | copy-start | bytes 24580
  10.5 361.7 %all-gather.19.cloned.1.call-start = ((), (), s32[]{:S(2)}) async-start(), calls=%async_computation.6 | async-start | bytes 2359296 | tf_op jit(solution)/shard_map/all_gather | solution.py:131
  11.3 411.9 %all-gather.25.cloned.1.call-start = ((), (), s32[]{:S(2)}) async-start(), calls=%async_computation.9 | async-start | bytes 2359296 | tf_op jit(solution)/shard_map/all_gather | solution.py:135
  12.0 424.2 %reduce-scatter.3.cloned.1.call-start = ((), (), s32[]{:S(2)}) async-start(), calls=%async_computation.10 | async-start | bytes 786432 | tf_op jit(solution)/shard_map/reduce_scatter | solution.py:162
  61.4 6.0 %copy-start.4 = (bf16[2048,512]{1,0:T(8,128)(2,1)S(1)}, bf16[2048,512]{1,0:T(8,128)(2,1)}, u32[]{:S(2)}) copy-start(bf16[2048,512]{1,0:T(8,128)(2,1)} %all-gather.13.cloned.1.call-done) | copy-start | bytes 6291460
  119.1 26.1 %copy-start.2 = (bf16[2048,512]{1,0:T(8,128)(2,1)S(1)}, bf16[2048,512]{1,0:T(8,128)(2,1)}, u32[]{:S(2)}) copy-start(bf16[2048,512]{1,0:T(8,128)(2,1)} %all-gather.11.cloned.1.call-done) | copy-start | bytes 6291460
  274.1 5.1 %copy-start.8 = (bf16[128,512]{1,0:T(8,128)(2,1)}, bf16[128,512]{1,0:T(8,128)(2,1)S(1)}, u32[]{:S(2)}) copy-start(bf16[128,512]{1,0:T(8,128)(2,1)S(1)} %fusion.21) | copy-start | bytes 393220
  274.1 4.2 copy-start.6
  274.1 4.2 copy-start.13
  274.1 52.9 %collective-permute-start = (bf16[2,512]{1,0:T(2,128)(2,1)S(1)}, bf16[2,512]{1,0:T(2,128)(2,1)S(1)}, u32[]{:S(2)}, u32[]{:S(2)}) collective-permute-start(bf16[2,512]{1,0:T(2,128)(2,1)S(1)} %slice.73), channel_id=1, source_target_pairs={{0,4},{4,8},{8,12},{1,5},{5,9},{9,13},{2,6},{6,10},{10,14},{3,7},{... | collective-permute-start | bytes 6152 | tf_op jit(solution)/shard_map/ppermute | solution.py:21
  279.3 46.5 %copy-start.1 = (bf16[2048,512]{1,0:T(8,128)(2,1)S(1)}, bf16[2048,512]{1,0:T(8,128)(2,1)}, u32[]{:S(2)}) copy-start(bf16[2048,512]{1,0:T(8,128)(2,1)} %all-gather.21.cloned.1.call-done) | copy-start | bytes 6291460
  423.2 4.5 copy-start
  427.6 3.4 copy-start.10
  427.6 17.4 %reduce-scatter.5.cloned.1.call-start = ((), (), s32[]{:S(2)}) async-start(), calls=%async_computation.11 | async-start | bytes 786432 | tf_op jit(solution)/shard_map/reduce_scatter | solution.py:162
  429.3 3.2 collective-permute-start.1
  (7 other events, 15.5 us)
Sparse Core Ops, SparseCore 0:
  9.5 51.8 all-gather.12
  63.5 53.3 all-gather.10
  119.0 50.9 all-gather.14
  172.0 49.9 all-gather.20
  223.9 48.0 all-gather.22
  273.9 48.8 all-gather.16
  324.9 47.2 all-gather.18
  374.3 48.8 all-gather.24
  427.7 6.1 reduce-scatter.2
  436.3 8.6 reduce-scatter.4
where the time goes:
time: 454 us
  waiting for transfers between devices  298 us (66%)
  blocking collectives  82.9 us (18%)
  matrix products  37.9 us (8%)
  between operations  14 us (3%)
  local copies, waits for them, and re-layouts  8.85 us (2%)
  other arithmetic  6.18 us (1%)
  starting transfers between devices  5.72 us (1%)
    all_gather x1, waiting for transfers between devices, on_device(): lax.all_gather(w_out_conv, ('sp', 'fs'), axis=1, tiled=True)  51 us
    all_gather x1, waiting for transfers between devices, on_device(): lax.all_gather(w_conv_in, ('sp', 'fs'), axis=0, tiled=True)  48 us
    all_gather x1, waiting for transfers between devices, on_device(): lax.all_gather(w_gate_b, ('sp', 'fs'), axis=0, tiled=True)  45.1 us
    all_gather x1, waiting for transfers between devices, on_device(): lax.all_gather(w_key, ('sp', 'fs'), axis=0, tiled=True)  44.2 us
    all_gather x1, waiting for transfers between devices, on_device(): lax.all_gather(w_out_attn, ('sp', 'fs'), axis=1, tiled=True)  42.6 us
    all_gather x2, blocking collectives, attend_heads(): lax.all_gather(key.reshape(rows, heads_here * 2 * DK), 'sp', axis=0, tile...  40.8 us
    all_gather x2, blocking collectives, attend_heads(): value_piece = lax.all_gather(value, 'sp', axis=0, tiled=True)  37.6 us
    all_gather x1, waiting for transfers between devices, on_device(): lax.all_gather(w_query, ('sp', 'fs'), axis=0, tiled=True)  24.1 us
  transfers between devices with their start and end apart: 12, of which 9 were waited for; matrix products, arithmetic and copies ran while one was open for 10% of the time, Pallas kernels for 0%

commit v1 on v0

--- a/solution.py
+++ b/solution.py
@@ -1,8 +1,11 @@
+import functools
 import math
 
 import jax
 import jax.numpy as jnp
 from jax import lax
+from jax.experimental import pallas as pl
+from jax.experimental.pallas import tpu as pltpu
 from jax.sharding import PartitionSpec as P
 
 DK = 64
@@ -106,7 +109,7 @@
     )
 
 
-def on_device(
+def gather_on_device(
     tokens,
     norm_gain,
     w_query,
@@ -172,6 +175,307 @@
     return jnp.stack(results, axis=0)
 
 
+MESH = pl.DeviceIdType.MESH
+
+
+def greet(peers):
+    barrier = pltpu.get_barrier_semaphore()
+    for peer in peers:
+        pl.semaphore_signal(barrier, inc=1, device_id=peer, device_id_type=MESH)
+    pl.semaphore_wait(barrier, len(peers))
+
+
+def remote(src, dst, send, recv, peer):
+    return pltpu.make_async_remote_copy(
+        src_ref=src, dst_ref=dst, send_sem=send, recv_sem=recv, device_id=peer, device_id_type=MESH
+    )
+
+
+def gather_kernel(
+    tok_ref, w_ref, o_ref, tok_all, w_all, o_all,
+    send_z, recv_z, send_t, recv_t, send_x, recv_x, send_y, recv_y, local,
+):
+    sp, fs = lax.axis_size("sp"), lax.axis_size("fs")
+    s, f = lax.axis_index("sp"), lax.axis_index("fs")
+    g, t = lax.axis_index("grp"), lax.axis_index("tp")
+    width = o_ref.shape[1]
+    z_peers = [{"sp": lax.rem(s + d, sp)} for d in range(1, sp)]
+    x_peers = [{"fs": lax.rem(f + d, fs)} for d in range(1, fs)]
+    y_peer = {"grp": 1 - g}
+    t_peer = {"tp": 1 - t}
+    greet(z_peers + x_peers + [y_peer, t_peer])
+
+    def tok_at(sv, tv):
+        return tok_all.at[:, sv * 2 + tv]
+
+    def w_at(gv, sv, fv):
+        return w_all.at[gv, sv * fs + fv]
+
+    def o_at(gv, sv, fv):
+        begin = pl.multiple_of((sv * fs + fv) * width, 128)
+        return o_all.at[gv, :, pl.ds(begin, width)]
+
+    started = []
+
+    def go(copy):
+        copy.start()
+        started.append(copy)
+
+    for d in range(1, sp):
+        to = lax.rem(s + d, sp)
+        peer = {"sp": to}
+        go(remote(tok_ref, tok_at(s, t), send_z.at[0, d], recv_z.at[0, d], peer))
+        go(remote(w_ref.at[to], w_at(g, s, f), send_z.at[1, d], recv_z.at[1, d], peer))
+        go(remote(o_ref, o_at(g, s, f), send_z.at[2, d], recv_z.at[2, d], peer))
+    keep = [
+        pltpu.make_async_copy(tok_ref, tok_at(s, t), local.at[0]),
+        pltpu.make_async_copy(w_ref.at[s], w_at(g, s, f), local.at[1]),
+        pltpu.make_async_copy(o_ref, o_at(g, s, f), local.at[2]),
+    ]
+    for copy in keep:
+        copy.start()
+
+    def z_wait(kind, d, ref):
+        remote(ref, ref, send_z.at[kind, d], recv_z.at[kind, d], t_peer).wait_recv()
+
+    for d in range(sp):
+        sv = lax.rem(s + sp - d, sp)
+        if d:
+            z_wait(0, d, tok_at(sv, t))
+        src = tok_at(sv, t) if d else tok_ref
+        go(remote(src, tok_at(sv, t), send_t.at[d], recv_t.at[d], t_peer))
+        if d:
+            z_wait(1, d, w_at(g, sv, f))
+        src = w_at(g, sv, f) if d else w_ref.at[s]
+        go(remote(src, w_at(g, sv, f), send_y.at[0, d], recv_y.at[0, d], y_peer))
+        for e, peer in enumerate(x_peers):
+            go(remote(src, w_at(g, sv, f), send_x.at[0, 0, d, e], recv_x.at[0, 0, d, e], peer))
+        if d:
+            z_wait(2, d, o_at(g, sv, f))
+        src = o_at(g, sv, f) if d else o_ref
+        go(remote(src, o_at(g, sv, f), send_y.at[1, d], recv_y.at[1, d], y_peer))
+        for e, peer in enumerate(x_peers):
+            go(remote(src, o_at(g, sv, f), send_x.at[1, 0, d, e], recv_x.at[1, 0, d, e], peer))
+    for d in range(sp):
+        sv = lax.rem(s + sp - d, sp)
+        for kind, at in enumerate((w_at, o_at)):
+            ref = at(1 - g, sv, f)
+            remote(ref, ref, send_y.at[kind, d], recv_y.at[kind, d], y_peer).wait_recv()
+            for e, peer in enumerate(x_peers):
+                go(remote(ref, ref, send_x.at[kind, 1, d, e], recv_x.at[kind, 1, d, e], peer))
+    for d in range(sp):
+        sv = lax.rem(s + sp - d, sp)
+        ref = tok_at(sv, 1 - t)
+        remote(ref, ref, send_t.at[d], recv_t.at[d], t_peer).wait_recv()
+        for kind, at in enumerate((w_at, o_at)):
+            for turn, gv in enumerate((g, 1 - g)):
+                for e in range(fs - 1):
+                    fv = lax.rem(f + fs - 1 - e, fs)
+                    ref = at(gv, sv, fv)
+                    remote(
+                        ref, ref, send_x.at[kind, turn, d, e], recv_x.at[kind, turn, d, e], t_peer
+                    ).wait_recv()
+    for copy in started:
+        copy.wait_send()
+    for copy in keep:
+        copy.wait()
+
+
+def gather_all(normed, w_half, o_half, sp, fs):
+    seqs, rows, wide = normed.shape
+    any_spec = pl.BlockSpec(memory_space=pl.ANY)
+    dma = pltpu.SemaphoreType.DMA
+    return pl.pallas_call(
+        gather_kernel,
+        out_shape=(
+            jax.ShapeDtypeStruct((seqs, sp * 2, rows, wide), jnp.bfloat16),
+            jax.ShapeDtypeStruct((2, sp * fs) + w_half.shape[1:], jnp.bfloat16),
+            jax.ShapeDtypeStruct((2, o_half.shape[0], o_half.shape[1] * sp * fs), jnp.bfloat16),
+        ),
+        in_specs=[any_spec] * 3,
+        out_specs=[any_spec] * 3,
+        scratch_shapes=[
+            dma((3, sp)), dma((3, sp)), dma((sp,)), dma((sp,)),
+            dma((2, 2, sp, fs - 1)), dma((2, 2, sp, fs - 1)),
+            dma((2, sp)), dma((2, sp)), dma((3,)),
+        ],
+        compiler_params=pltpu.CompilerParams(collective_id=0, has_side_effects=True),
+        name="gather_all",
+    )(normed, w_half, o_half)
+
+
+def merge_kernel(
+    attn_ref, conv_ref, o_ref, out_ref, feats, weights, mine, theirs, got, send, recv, swap, local,
+):
+    sp = lax.axis_size("sp")
+    s, t = lax.axis_index("sp"), lax.axis_index("tp")
+    z_peers = [{"sp": lax.rem(s + d, sp)} for d in range(1, sp)]
+    t_peer = {"tp": 1 - t}
+    greet(z_peers + [t_peer])
+    seqs, unused, rows, wide = attn_ref.shape
+    fetch = pltpu.make_async_copy(o_ref, weights, local.at[2])
+    started = []
+    for d in range(1, sp):
+        to = lax.rem(s + d, sp)
+        for kind, ref in enumerate((attn_ref, conv_ref)):
+            copy = remote(
+                ref.at[:, to], feats.at[kind, s], send.at[kind, d], recv.at[kind, d], {"sp": to}
+            )
+            copy.start()
+            started.append(copy)
+    fetch.start()
+    keep = [
+        pltpu.make_async_copy(ref.at[:, s], feats.at[kind, s], local.at[kind])
+        for kind, ref in enumerate((attn_ref, conv_ref))
+    ]
+    for copy in keep:
+        copy.start()
+    for copy in keep:
+        copy.wait()
+    for copy in started:
+        copy.wait()
+    fetch.wait()
+    half = rows // 2
+    piece = 512 if weights.shape[2] % 512 == 0 else weights.shape[2]
+
+    def product(tv, begin):
+        total = jnp.zeros((seqs * half, piece), jnp.float32)
+        for kind in range(2):
+            left = jnp.concatenate(
+                [
+                    feats[kind, sv, :, pl.ds(pl.multiple_of(tv * half, half), half), :].reshape(
+                        seqs * half, wide
+                    )
+                    for sv in range(sp)
+                ],
+                axis=1,
+            )
+            total = total + jnp.dot(
+                left, weights[kind, :, pl.ds(begin, piece)], preferred_element_type=jnp.float32
+            )
+        return total
+
+    copies = []
+    for turn in range(weights.shape[2] // piece):
+        theirs[turn] = product(1 - t, turn * piece).astype(jnp.bfloat16)
+        copy = remote(theirs.at[turn], got.at[turn], swap.at[0, turn], swap.at[1, turn], t_peer)
+        copy.start()
+        copies.append(copy)
+    for turn in range(weights.shape[2] // piece):
+        mine[turn] = product(t, turn * piece)
+    for turn, copy in enumerate(copies):
+        copy.wait()
+        total = mine[turn] + got[turn].astype(jnp.float32)
+        out_ref[:, :, pl.ds(turn * piece, piece)] = total.astype(jnp.bfloat16).reshape(
+            seqs, half, piece
+        )
+
+
+def merge(attn, conv_out, o_all):
+    seqs, sp, rows, wide = attn.shape
+    columns = o_all.shape[2]
+    piece = 512 if columns % 512 == 0 else columns
+    turns = columns // piece
+    half = rows // 2
+    any_spec = pl.BlockSpec(memory_space=pl.ANY)
+    dma = pltpu.SemaphoreType.DMA
+    return pl.pallas_call(
+        merge_kernel,
+        out_shape=jax.ShapeDtypeStruct((seqs, half, columns), jnp.bfloat16),
+        in_specs=[any_spec] * 3,
+        out_specs=pl.BlockSpec(memory_space=pltpu.VMEM),
+        scratch_shapes=[
+            pltpu.VMEM((2, sp, seqs, rows, wide), jnp.bfloat16),
+            pltpu.VMEM(o_all.shape, jnp.bfloat16),
+            pltpu.VMEM((turns, seqs * half, piece), jnp.float32),
+            pltpu.VMEM((turns, seqs * half, piece), jnp.bfloat16),
+            pltpu.VMEM((turns, seqs * half, piece), jnp.bfloat16),
+            dma((2, sp)), dma((2, sp)), dma((2, turns)), dma((3,)),
+        ],
+        compiler_params=pltpu.CompilerParams(collective_id=1, has_side_effects=True),
+        name="merge",
+    )(attn, conv_out, o_all)
+
+
+def head_map(query, key, value, mix, head_gain):
+    seqs, count = value.shape[0], value.shape[1]
+    score = jnp.einsum("bqmd,bkmd->bmqk", query, key, preferred_element_type=jnp.float32)
+    score = score * DK ** (-0.5)
+    place = jnp.arange(count, dtype=jnp.int32)
+    score = jnp.where(place[None, :] <= place[:, None], score, NEG)
+    weights = jnp.exp(score - jnp.max(score, axis=-1, keepdims=True))
+    total = jnp.sum(weights, axis=-1)
+    summed = jnp.einsum(
+        "bmqk,bkd->bmqd", weights.astype(jnp.bfloat16), value, preferred_element_type=jnp.float32
+    )
+    mapped = summed / total[..., None]
+    return (rms_scale(mapped[:, 0] - mix * mapped[:, 1], head_gain) * OUT_SCALE).astype(jnp.bfloat16)
+
+
+def heads_on_device(
+    tokens, norm_gain, w_query, w_key, w_value, query_gain, key_gain, mix_lambda, head_gain,
+    w_gate_b, w_gate_c, w_conv_in, conv_taps, w_out_attn, w_out_conv,
+):
+    sp, fs = lax.axis_size("sp"), lax.axis_size("fs")
+    s, first = lax.axis_index("sp"), lax.axis_index("grp") == 0
+    seqs, rows, wide = tokens.shape
+    normed = rms_scale(tokens, norm_gain).astype(jnp.bfloat16)
+    depth, columns = w_query.shape
+    each = columns // sp
+
+    def half(pair):
+        return jnp.where(first, pair[0], pair[1])
+
+    picked = [
+        half(pair).reshape(depth, sp, each)
+        for pair in ((w_query, w_gate_b), (w_key, w_gate_c), (w_value, w_conv_in))
+    ]
+    w_half = jnp.stack(picked, axis=2).transpose(1, 0, 2, 3).reshape(sp, depth, 3 * each)
+    o_half = half((w_out_attn, w_out_conv))
+    tok_all, w_all, o_all = gather_all(normed, w_half, o_half, sp, fs)
+    count = rows * sp * 2
+    x = tok_all.reshape(seqs * count, wide)
+
+    def project(index):
+        out = jnp.dot(
+            x, w_all[index].reshape(wide, 3 * each), preferred_element_type=jnp.float32
+        ).astype(jnp.bfloat16)
+        return [out[:, n * each : (n + 1) * each].reshape(seqs, count, each) for n in range(3)]
+
+    query_raw, key_raw, value = project(0)
+    gate_b, gate_c, conv_in = project(1)
+
+    def mine(array, axis=0):
+        return lax.dynamic_slice_in_dim(array, s * each, each, axis)
+
+    query = rms_scale(
+        query_raw.reshape(seqs, count, 2, DK), mine(query_gain).reshape(2, DK)
+    ).astype(jnp.bfloat16)
+    key = rms_scale(
+        key_raw.reshape(seqs, count, 2, DK), mine(key_gain).reshape(2, DK)
+    ).astype(jnp.bfloat16)
+    mix = lax.dynamic_slice_in_dim(mix_lambda, s, 1)[0]
+    attn = head_map(query, key, value, mix, head_gain)
+    shaped = (gate_c.astype(jnp.float32) * conv_in.astype(jnp.float32)).astype(jnp.bfloat16)
+    padded = jnp.pad(shaped, ((0, 0), (KW - 1, 0), (0, 0))).astype(jnp.float32)
+    taps = mine(conv_taps, 1)
+    conv = taps[0] * padded[:, 0:count]
+    for tap in range(1, KW):
+        conv = conv + taps[tap] * padded[:, tap : tap + count]
+    conv_out = (gate_b.astype(jnp.float32) * conv).astype(jnp.bfloat16)
+    shape = (seqs, sp, rows * 2, each)
+    return merge(attn.reshape(shape), conv_out.reshape(shape), o_all)
+
+
+def on_device(*arrays):
+    heads_here, channels = arrays[7].shape[0], arrays[12].shape[1]
+    sizes = [lax.axis_size(axis) for axis in ("grp", "tp", "fs", "sp")]
+    whole_heads = heads_here == sizes[3] and channels == heads_here * DV
+    if whole_heads and sizes[0] == 2 and sizes[1] == 2 and sizes[2] > 1:
+        return heads_on_device(*arrays)
+    return gather_on_device(*arrays)
+
+
 def solution(mesh):
     placed = (
         P(("grp", "fs"), ("sp", "tp"), None),

time: 454 us -> 193 us (0.43)
  waiting for transfers between devices: 298 us -> 0 us
  Pallas kernels: 0 us -> 163 us
  blocking collectives: 82.9 us -> 0 us
  matrix products: 37.9 us -> 9.61 us
  between operations: 14 us -> 0.28 us
  starting transfers between devices: 5.72 us -> 0 us
    all_gather x8 -> x0, waiting for transfers between devices: 284 us -> none  [the longest x1 51 us: on_device(): lax.all_gather(w_out_conv, ('sp', 'fs'), axis=1, tiled=True)]
    pallas_call x0 -> x2, Pallas kernels: none -> 163 us  [the longest x1 127 us: gather_all(): pl.pallas_call(gather_kernel, out_shape=(jax.ShapeDtypeStruct((seqs, sp *...]
    all_gather x6 -> x0, blocking collectives: 82.9 us -> none  [the longest x2 40.8 us: attend_heads(): lax.all_gather(key.reshape(rows, heads_here * 2 * DK), 'sp', axis=0, tile...]
    dot_general x18 -> x4, matrix products: 37.9 us -> 9.61 us  [the longest x2 6.83 us: project(): jnp.dot(x, w_all[index].reshape(wide, 3 * each), preferred_element_type=j...]
    reduce_scatter x2 -> x0, waiting for transfers between devices: 8.86 us -> none  [on_device(): lax.psum_scatter((jnp.dot(attn, out_attn, preferred_element_type=jnp.floa...]
    ppermute x2 -> x0, starting transfers between devices: 5.37 us -> none  [from_behind(): return lax.ppermute(block, axis, route)]
    unnamed x10 -> x0, waiting for transfers between devices: 5.09 us -> none
  transfers between devices with their start and end apart: 12 -> 0, of which waited for: 9 -> 0; matrix products, arithmetic and copies ran while one was open for 10% -> 0% of each run, Pallas kernels for 0% -> 0%
where the time goes in v1:
time: 193 us; the launch traced here: 192 us
  Pallas kernels  163 us (84%)
  local copies, waits for them, and re-layouts  10.2 us (5%)
  matrix products  9.61 us (5%)
  other arithmetic  9.14 us (5%)
    pallas_call x1, Pallas kernels, gather_all(): pl.pallas_call(gather_kernel, out_shape=(jax.ShapeDtypeStruct((seqs, sp *...  127 us
    pallas_call x1, Pallas kernels, merge(): pl.pallas_call(merge_kernel, out_shape=jax.ShapeDtypeStruct((seqs, half,...  36.1 us
    dot_general x2, matrix products, project(): jnp.dot(x, w_all[index].reshape(wide, 3 * each), preferred_element_type=j...  6.83 us

profile of v1, /device:TPU:0, one launch (start us, length us, event | category | flops | bytes accessed | tf_op | source)
XLA Modules:
  0.0 192.4 jit_solution(7397817456374448183)
XLA Ops:
  0.0 1.2 broadcast_select_fusion.1
  1.5 1.0 broadcast_select_fusion.3
  2.7 1.2 copy.25.w_ref
  3.9 0.7 broadcast_select_fusion.o_ref
  4.8 1.0 fusion.11.tok_ref
  5.8 127.0 %gather_all.1 = (bf16[2,8,64,2048]{3,2,1,0:T(8,128)(2,1)}, bf16[2,8,256,384]{3,2,1,0:T(8,128)(2,1)}, bf16[2,512,2048]{2,1,0:T(8,128)(2,1)}) custom-call(bf16[2,64,2048]{2,1,0:T(8,128)(2,1)} %fusion.11.tok_ref, bf16[4,256,384]{2,1,0:T(8,128)(2,1)} %copy.25.w_ref, bf16[512,256]{1,0:T(8,128)(2,1)} %broadcast_select_fusion.o_ref), custom_call_target="tpu_custom_call" | custom-call | tf_op jit(solution)/shard_map/gather_all/pallas_call | solution.py:288
  132.8 2.4 %fusion.26 = (bf16[1,8,256,384]{3,2,1,0:T(8,128)(2,1)S(1)}, bf16[1,8,256,384]{3,2,1,0:T(8,128)(2,1)S(1)}) fusion(bf16[2,8,256,384]{3,2,1,0:T(8,128)(2,1)} %get-tuple-element.9), kind=kLoop, calls=%fused_computation.56 | loop fusion | bytes 6291456 | tf_op jit(solution)/shard_map/slice | solution.py:441
  135.2 0.7 copy-done.6
  136.0 2.3 %convolution_convert_fusion = bf16[1024,384]{1,0:T(8,128)(2,1)S(1)} fusion(bf16[1024,2048]{1,0:T(8,128)(2,1)S(1)} %bitcast.47, bf16[2048,384]{1,0:T(8,128)(2,1)S(1)} %bitcast.38), kind=kOutput, calls=%fused_computation.10 | convolution fusion | flops 1611005952 | bytes 6553600 | tf_op jit(solution)/shard_map/dot_general | solution.py:440
  138.5 0.9 fusion.17
  139.4 4.5 %convolution_convert_fusion.1 = bf16[1024,384]{1,0:T(8,128)(2,1)S(1)} fusion(bf16[1024,2048]{1,0:T(8,128)(2,1)} %bitcast.46, bf16[2048,384]{1,0:T(8,128)(2,1)S(1)} %bitcast.37), kind=kOutput, calls=%fused_computation.11 | convolution fusion | flops 1611005952 | bytes 6553600 | tf_op jit(solution)/shard_map/dot_general | solution.py:440
  144.3 0.4 reshape.88
  144.9 0.8 dynamic_slice.12
  145.8 0.3 multiply_convert_fusion.3
  146.3 0.4 reshape.89
  147.0 0.8 dynamic_slice.13
  148.2 0.9 fusion
  149.1 0.9 fusion.1
  150.1 1.8 fusion.12
  151.9 0.6 dynamic_slice.14
  152.5 0.9 multiply_reduce_fusion
  153.4 0.9 multiply_convert_fusion.1.attn_ref
  154.3 36.1 %merge.1 = bf16[2,64,2048]{2,1,0:T(8,128)(2,1)} custom-call(bf16[2,4,128,128]{3,2,1,0:T(8,128)(2,1)} %multiply_convert_fusion.1.attn_ref, bf16[2,4,128,128]{3,2,1,0:T(8,128)(2,1)} %bitcast.39, bf16[2,512,2048]{2,1,0:T(8,128)(2,1)} %get-tuple-element.10.o_ref), custom_call_target="tpu_custom_call" | custom-call | tf_op jit(solution)/shard_map/merge/pallas_call | solution.py:382
  190.5 1.9 copy.42
  (39 shorter events, 2.4 us)
Async XLA Ops:
  0.0 138.5 %copy-start = (f32[3,512]{1,0:T(4,128)S(1)}, f32[3,512]{1,0:T(4,128)}, u32[]{:S(2)}) copy-start(f32[3,512]{1,0:T(4,128)} %param.27) | copy-start | bytes 18436
  0.0 3.9 %copy-start.2 = (bf16[512,256]{1,0:T(8,128)(2,1)S(1)}, bf16[512,256]{1,0:T(8,128)(2,1)}, u32[]{:S(2)}) copy-start(bf16[512,256]{1,0:T(8,128)(2,1)} %param.28) | copy-start | bytes 786436
  0.0 3.9 %copy-start.3 = (bf16[512,256]{1,0:T(8,128)(2,1)S(1)}, bf16[512,256]{1,0:T(8,128)(2,1)}, u32[]{:S(2)}) copy-start(bf16[512,256]{1,0:T(8,128)(2,1)} %param.29) | copy-start | bytes 786436
  0.0 4.6 %copy-start.1 = (bf16[2,64,2048]{2,1,0:T(8,128)(2,1)S(1)}, bf16[2,64,2048]{2,1,0:T(8,128)(2,1)}, u32[]{:S(2)}) copy-start(bf16[2,64,2048]{2,1,0:T(8,128)(2,1)} %param.15) | copy-start | bytes 1572868
  0.0 4.8 %copy-start.4 = (f32[2048]{0:T(1024)S(1)}, f32[2048]{0:T(1024)}, u32[]{:S(2)}) copy-start(f32[2048]{0:T(1024)} %param.16) | copy-start | bytes 24580
  132.8 3.1 %copy-start.6 = (bf16[2,8,64,2048]{3,2,1,0:T(8,128)(2,1)S(1)}, bf16[2,8,64,2048]{3,2,1,0:T(8,128)(2,1)}, u32[]{:S(2)}) copy-start(bf16[2,8,64,2048]{3,2,1,0:T(8,128)(2,1)} %get-tuple-element.8) | copy-start | bytes 12582916
  150.0 1.9 copy-start.7
  150.0 3.4 %copy-start.5 = (f32[128]{0:T(128)S(1)}, f32[128]{0:T(128)}, u32[]{:S(2)}) copy-start(f32[128]{0:T(128)} %param.23) | copy-start | bytes 1540

commit v2 on v1

--- a/solution.py
+++ b/solution.py
@@ -193,7 +193,7 @@
 
 def gather_kernel(
     tok_ref, w_ref, o_ref, tok_all, w_all, o_all,
-    send_z, recv_z, send_t, recv_t, send_x, recv_x, send_y, recv_y, local,
+    send_z, recv_z, send_c, recv_c, send_t, recv_t, send_x, recv_x, send_y, recv_y, local,
 ):
     sp, fs = lax.axis_size("sp"), lax.axis_size("fs")
     s, f = lax.axis_index("sp"), lax.axis_index("fs")
@@ -211,72 +211,114 @@
     def w_at(gv, sv, fv):
         return w_all.at[gv, sv * fs + fv]
 
-    def o_at(gv, sv, fv):
-        begin = pl.multiple_of((sv * fs + fv) * width, 128)
-        return o_all.at[gv, :, pl.ds(begin, width)]
+    def o_at(gv, sv):
+        return o_all.at[gv, :, pl.ds(pl.multiple_of(sv * width, 128), width)]
 
     started = []
 
-    def go(copy):
-        copy.start()
-        started.append(copy)
+    def go(copy, needs=()):
+        def run(act):
+            if needs:
+                pl.when(functools.reduce(jnp.logical_and, needs))(act)
+            else:
+                act()
+
+        run(copy.start)
+        started.append((run, copy))
+
+    def arrived(sem, ref, needs=()):
+        copy = remote(ref, ref, sem, sem, t_peer)
+        if needs:
+            pl.when(functools.reduce(jnp.logical_and, needs))(copy.wait_recv)
+        else:
+            copy.wait_recv()
+
+    def chain(kind, at, src, sv, needs):
+        ref = at(sv)
+        for way, (to, moves) in enumerate(((s + 1, sv <= s), (s - 1, sv >= s))):
+            fits = to < sp if way == 0 else to >= 0
+            peer = {"sp": jnp.clip(to, 0, sp - 1)}
+            go(
+                remote(src, ref, send_c.at[kind, way, sv], recv_c.at[kind, sv], peer),
+                needs + [fits, moves],
+            )
+
+    def spread_w(d, src):
+        sv = lax.rem(s + sp - d, sp)
+        for e, peer in enumerate(x_peers):
+            go(remote(src, w_at(g, sv, f), send_x.at[0, d, e], recv_x.at[0, d, e], peer))
+        go(remote(src, w_at(g, sv, f), send_y.at[0, d], recv_y.at[0, d], y_peer))
+
+    def tok_mine(sv):
+        return tok_at(sv, t)
+
+    def o_mine(sv):
+        return o_at(g, sv)
 
     for d in range(1, sp):
         to = lax.rem(s + d, sp)
-        peer = {"sp": to}
-        go(remote(tok_ref, tok_at(s, t), send_z.at[0, d], recv_z.at[0, d], peer))
-        go(remote(w_ref.at[to], w_at(g, s, f), send_z.at[1, d], recv_z.at[1, d], peer))
-        go(remote(o_ref, o_at(g, s, f), send_z.at[2, d], recv_z.at[2, d], peer))
+        go(remote(w_ref.at[to], w_at(g, s, f), send_z.at[d], recv_z.at[d], {"sp": to}))
+    chain(0, tok_mine, tok_ref, s, [])
+    spread_w(0, w_ref.at[s])
+    go(remote(tok_ref, tok_mine(s), send_t.at[s], recv_t.at[s], t_peer))
     keep = [
         pltpu.make_async_copy(tok_ref, tok_at(s, t), local.at[0]),
         pltpu.make_async_copy(w_ref.at[s], w_at(g, s, f), local.at[1]),
-        pltpu.make_async_copy(o_ref, o_at(g, s, f), local.at[2]),
+        pltpu.make_async_copy(o_ref, o_at(g, s), local.at[2]),
     ]
     for copy in keep:
         copy.start()
-
-    def z_wait(kind, d, ref):
-        remote(ref, ref, send_z.at[kind, d], recv_z.at[kind, d], t_peer).wait_recv()
-
+    for d in range(1, sp):
+        ref = w_at(g, lax.rem(s + sp - d, sp), f)
+        arrived(recv_z.at[d], ref)
+        spread_w(d, ref)
+
+    def around(kind, at, distance, beyond):
+        for shift in (-distance, distance):
+            sv = jnp.clip(s + shift, 0, sp - 1)
+            there = (s + shift >= 0) if shift < 0 else (s + shift < sp)
+            ref = at(sv)
+            arrived(recv_c.at[kind, sv], ref, [there])
+            if shift < 0:
+                to, fits, way = s + 1, s + 1 < sp, 0
+            else:
+                to, fits, way = s - 1, s - 1 >= 0, 1
+            peer = {"sp": jnp.clip(to, 0, sp - 1)}
+            go(
+                remote(ref, ref, send_c.at[kind, way, sv], recv_c.at[kind, sv], peer),
+                [there, fits],
+            )
+            beyond(sv, ref, there)
+
+    def tok_beyond(sv, ref, there):
+        go(remote(ref, ref, send_t.at[sv], recv_t.at[sv], t_peer), [there])
+
+    def o_beyond(sv, ref, there):
+        go(remote(ref, ref, send_y.at[1, sv], recv_y.at[1, sv], y_peer), [there])
+
+    for k in range(1, sp):
+        around(0, tok_mine, k, tok_beyond)
+        if k == 1:
+            for d in range(sp):
+                ref = w_at(1 - g, lax.rem(s + sp - d, sp), f)
+                arrived(recv_y.at[0, d], ref)
+                for e, peer in enumerate(x_peers):
+                    go(remote(ref, ref, send_x.at[1, d, e], recv_x.at[1, d, e], peer))
+            chain(1, o_mine, o_ref, s, [])
+            go(remote(o_ref, o_mine(s), send_y.at[1, s], recv_y.at[1, s], y_peer))
+    for k in range(1, sp):
+        around(1, o_mine, k, o_beyond)
+    for sv in range(sp):
+        arrived(recv_t.at[sv], tok_at(sv, 1 - t))
+        arrived(recv_y.at[1, sv], o_at(1 - g, sv))
     for d in range(sp):
         sv = lax.rem(s + sp - d, sp)
-        if d:
-            z_wait(0, d, tok_at(sv, t))
-        src = tok_at(sv, t) if d else tok_ref
-        go(remote(src, tok_at(sv, t), send_t.at[d], recv_t.at[d], t_peer))
-        if d:
-            z_wait(1, d, w_at(g, sv, f))
-        src = w_at(g, sv, f) if d else w_ref.at[s]
-        go(remote(src, w_at(g, sv, f), send_y.at[0, d], recv_y.at[0, d], y_peer))
-        for e, peer in enumerate(x_peers):
-            go(remote(src, w_at(g, sv, f), send_x.at[0, 0, d, e], recv_x.at[0, 0, d, e], peer))
-        if d:
-            z_wait(2, d, o_at(g, sv, f))
-        src = o_at(g, sv, f) if d else o_ref
-        go(remote(src, o_at(g, sv, f), send_y.at[1, d], recv_y.at[1, d], y_peer))
-        for e, peer in enumerate(x_peers):
-            go(remote(src, o_at(g, sv, f), send_x.at[1, 0, d, e], recv_x.at[1, 0, d, e], peer))
-    for d in range(sp):
-        sv = lax.rem(s + sp - d, sp)
-        for kind, at in enumerate((w_at, o_at)):
-            ref = at(1 - g, sv, f)
-            remote(ref, ref, send_y.at[kind, d], recv_y.at[kind, d], y_peer).wait_recv()
-            for e, peer in enumerate(x_peers):
-                go(remote(ref, ref, send_x.at[kind, 1, d, e], recv_x.at[kind, 1, d, e], peer))
-    for d in range(sp):
-        sv = lax.rem(s + sp - d, sp)
-        ref = tok_at(sv, 1 - t)
-        remote(ref, ref, send_t.at[d], recv_t.at[d], t_peer).wait_recv()
-        for kind, at in enumerate((w_at, o_at)):
-            for turn, gv in enumerate((g, 1 - g)):
-                for e in range(fs - 1):
-                    fv = lax.rem(f + fs - 1 - e, fs)
-                    ref = at(gv, sv, fv)
-                    remote(
-                        ref, ref, send_x.at[kind, turn, d, e], recv_x.at[kind, turn, d, e], t_peer
-                    ).wait_recv()
-    for copy in started:
-        copy.wait_send()
+        for turn, gv in enumerate((g, 1 - g)):
+            for e in range(fs - 1):
+                fv = lax.rem(f + fs - 1 - e, fs)
+                arrived(recv_x.at[turn, d, e], w_at(gv, sv, fv))
+    for run, copy in started:
+        run(copy.wait_send)
     for copy in keep:
         copy.wait()
 
@@ -290,14 +332,13 @@
         out_shape=(
             jax.ShapeDtypeStruct((seqs, sp * 2, rows, wide), jnp.bfloat16),
             jax.ShapeDtypeStruct((2, sp * fs) + w_half.shape[1:], jnp.bfloat16),
-            jax.ShapeDtypeStruct((2, o_half.shape[0], o_half.shape[1] * sp * fs), jnp.bfloat16),
+            jax.ShapeDtypeStruct((2, o_half.shape[0], o_half.shape[1] * sp), jnp.bfloat16),
         ),
         in_specs=[any_spec] * 3,
         out_specs=[any_spec] * 3,
         scratch_shapes=[
-            dma((3, sp)), dma((3, sp)), dma((sp,)), dma((sp,)),
-            dma((2, 2, sp, fs - 1)), dma((2, 2, sp, fs - 1)),
-            dma((2, sp)), dma((2, sp)), dma((3,)),
+            dma((sp,)), dma((sp,)), dma((2, 2, sp)), dma((2, sp)), dma((sp,)), dma((sp,)),
+            dma((2, sp, fs - 1)), dma((2, sp, fs - 1)), dma((2, sp)), dma((2, sp)), dma((3,)),
         ],
         compiler_params=pltpu.CompilerParams(collective_id=0, has_side_effects=True),
         name="gather_all",
@@ -305,96 +346,142 @@
 
 
 def merge_kernel(
-    attn_ref, conv_ref, o_ref, out_ref, feats, weights, mine, theirs, got, send, recv, swap, local,
+    attn_ref, conv_ref, o_ref, out_ref, feats, weights, mine, theirs, got, done, landed,
+    send, recv, send_x, recv_x, swap, last, local,
 ):
-    sp = lax.axis_size("sp")
-    s, t = lax.axis_index("sp"), lax.axis_index("tp")
+    sp, fs = lax.axis_size("sp"), lax.axis_size("fs")
+    s, t, f = lax.axis_index("sp"), lax.axis_index("tp"), lax.axis_index("fs")
     z_peers = [{"sp": lax.rem(s + d, sp)} for d in range(1, sp)]
+    x_peers = [{"fs": lax.rem(f + d, fs)} for d in range(1, fs)]
     t_peer = {"tp": 1 - t}
-    greet(z_peers + [t_peer])
+    greet(z_peers + x_peers + [t_peer])
     seqs, unused, rows, wide = attn_ref.shape
-    fetch = pltpu.make_async_copy(o_ref, weights, local.at[2])
+    half = rows // 2
+    refs = (attn_ref, conv_ref)
     started = []
+
+    def go(copy):
+        copy.start()
+        started.append(copy)
+        return copy
+
     for d in range(1, sp):
         to = lax.rem(s + d, sp)
-        for kind, ref in enumerate((attn_ref, conv_ref)):
-            copy = remote(
-                ref.at[:, to], feats.at[kind, s], send.at[kind, d], recv.at[kind, d], {"sp": to}
-            )
-            copy.start()
-            started.append(copy)
+        for kind, ref in enumerate(refs):
+            go(
+                remote(
+                    ref.at[:, to], feats.at[f, kind, s], send.at[kind, d], recv.at[kind, d],
+                    {"sp": to},
+                )
+            )
+    for kind, ref in enumerate(refs):
+        for e, peer in enumerate(x_peers):
+            go(
+                remote(
+                    ref.at[:, s], feats.at[f, kind, s], send_x.at[kind, 0, e],
+                    recv_x.at[kind, 0, e], peer,
+                )
+            )
+    fetch = pltpu.make_async_copy(o_ref, weights, local.at[2])
     fetch.start()
     keep = [
-        pltpu.make_async_copy(ref.at[:, s], feats.at[kind, s], local.at[kind])
-        for kind, ref in enumerate((attn_ref, conv_ref))
+        pltpu.make_async_copy(ref.at[:, s], feats.at[f, kind, s], local.at[kind])
+        for kind, ref in enumerate(refs)
     ]
     for copy in keep:
         copy.start()
+    for d in range(1, sp):
+        sv = lax.rem(s + sp - d, sp)
+        for kind in range(2):
+            ref = feats.at[f, kind, sv]
+            remote(ref, ref, send.at[kind, d], recv.at[kind, d], t_peer).wait_recv()
+            for e, peer in enumerate(x_peers):
+                go(remote(ref, ref, send_x.at[kind, d, e], recv_x.at[kind, d, e], peer))
     for copy in keep:
         copy.wait()
-    for copy in started:
-        copy.wait()
     fetch.wait()
-    half = rows // 2
-    piece = 512 if weights.shape[2] % 512 == 0 else weights.shape[2]
-
-    def product(tv, begin):
-        total = jnp.zeros((seqs * half, piece), jnp.float32)
+
+    def product(fv, tv):
+        total = jnp.zeros((seqs * half, weights.shape[2]), jnp.float32)
         for kind in range(2):
             left = jnp.concatenate(
                 [
-                    feats[kind, sv, :, pl.ds(pl.multiple_of(tv * half, half), half), :].reshape(
+                    feats[fv, kind, sv, :, pl.ds(pl.multiple_of(tv * half, half), half), :].reshape(
                         seqs * half, wide
                     )
                     for sv in range(sp)
                 ],
                 axis=1,
             )
-            total = total + jnp.dot(
-                left, weights[kind, :, pl.ds(begin, piece)], preferred_element_type=jnp.float32
-            )
+            total = total + jnp.dot(left, weights[kind], preferred_element_type=jnp.float32)
         return total
 
-    copies = []
-    for turn in range(weights.shape[2] // piece):
-        theirs[turn] = product(1 - t, turn * piece).astype(jnp.bfloat16)
-        copy = remote(theirs.at[turn], got.at[turn], swap.at[0, turn], swap.at[1, turn], t_peer)
-        copy.start()
-        copies.append(copy)
-    for turn in range(weights.shape[2] // piece):
-        mine[turn] = product(t, turn * piece)
-    for turn, copy in enumerate(copies):
-        copy.wait()
-        total = mine[turn] + got[turn].astype(jnp.float32)
-        out_ref[:, :, pl.ds(turn * piece, piece)] = total.astype(jnp.bfloat16).reshape(
-            seqs, half, piece
+    swaps, lasts = [], []
+    for e in range(fs):
+        fv = lax.rem(f + e, fs)
+        if e:
+            for d in range(sp):
+                sv = lax.rem(s + sp - d, sp)
+                for kind in range(2):
+                    ref = feats.at[fv, kind, sv]
+                    remote(
+                        ref, ref, send_x.at[kind, d, fs - 1 - e], recv_x.at[kind, d, fs - 1 - e],
+                        t_peer,
+                    ).wait_recv()
+        theirs[e] = product(fv, 1 - t).astype(jnp.bfloat16)
+        swaps.append(
+            go(remote(theirs.at[e], got.at[e], swap.at[0, e], swap.at[1, e], t_peer))
         )
-
-
-def merge(attn, conv_out, o_all):
+        mine[e] = product(fv, t)
+    for e in list(range(1, fs)) + [0]:
+        swaps[e].wait_recv()
+        total = (mine[e] + got[e].astype(jnp.float32)).astype(jnp.bfloat16)
+        if e:
+            done[e - 1] = total
+            lasts.append(
+                go(
+                    remote(
+                        done.at[e - 1], landed.at[e - 1], last.at[0, e - 1], last.at[1, e - 1],
+                        x_peers[e - 1],
+                    )
+                )
+            )
+        else:
+            out_ref[f] = total
+    for e in range(1, fs):
+        lasts[e - 1].wait_recv()
+        out_ref[lax.rem(f + fs - e, fs)] = landed[e - 1]
+    for copy in started:
+        copy.wait_send()
+
+
+def merge(attn, conv_out, o_all, fs):
     seqs, sp, rows, wide = attn.shape
     columns = o_all.shape[2]
-    piece = 512 if columns % 512 == 0 else columns
-    turns = columns // piece
-    half = rows // 2
+    lines = seqs * (rows // 2)
     any_spec = pl.BlockSpec(memory_space=pl.ANY)
     dma = pltpu.SemaphoreType.DMA
-    return pl.pallas_call(
+    out = pl.pallas_call(
         merge_kernel,
-        out_shape=jax.ShapeDtypeStruct((seqs, half, columns), jnp.bfloat16),
+        out_shape=jax.ShapeDtypeStruct((fs, lines, columns), jnp.bfloat16),
         in_specs=[any_spec] * 3,
         out_specs=pl.BlockSpec(memory_space=pltpu.VMEM),
         scratch_shapes=[
-            pltpu.VMEM((2, sp, seqs, rows, wide), jnp.bfloat16),
+            pltpu.VMEM((fs, 2, sp, seqs, rows, wide), jnp.bfloat16),
             pltpu.VMEM(o_all.shape, jnp.bfloat16),
-            pltpu.VMEM((turns, seqs * half, piece), jnp.float32),
-            pltpu.VMEM((turns, seqs * half, piece), jnp.bfloat16),
-            pltpu.VMEM((turns, seqs * half, piece), jnp.bfloat16),
-            dma((2, sp)), dma((2, sp)), dma((2, turns)), dma((3,)),
+            pltpu.VMEM((fs, lines, columns), jnp.float32),
+            pltpu.VMEM((fs, lines, columns), jnp.bfloat16),
+            pltpu.VMEM((fs, lines, columns), jnp.bfloat16),
+            pltpu.VMEM((fs - 1, lines, columns), jnp.bfloat16),
+            pltpu.VMEM((fs - 1, lines, columns), jnp.bfloat16),
+            dma((2, sp)), dma((2, sp)), dma((2, sp, fs - 1)), dma((2, sp, fs - 1)),
+            dma((2, fs)), dma((2, fs - 1)), dma((3,)),
         ],
         compiler_params=pltpu.CompilerParams(collective_id=1, has_side_effects=True),
         name="merge",
     )(attn, conv_out, o_all)
+    out = out.reshape(fs, lines, sp, columns // sp).transpose(1, 2, 0, 3)
+    return out.reshape(seqs, rows // 2, fs * columns)
 
 
 def head_map(query, key, value, mix, head_gain):
@@ -464,7 +551,7 @@
         conv = conv + taps[tap] * padded[:, tap : tap + count]
     conv_out = (gate_b.astype(jnp.float32) * conv).astype(jnp.bfloat16)
     shape = (seqs, sp, rows * 2, each)
-    return merge(attn.reshape(shape), conv_out.reshape(shape), o_all)
+    return merge(attn.reshape(shape), conv_out.reshape(shape), o_all, fs)
 
 
 def on_device(*arrays):

time: 193 us -> 141 us (0.73)
  Pallas kernels: 163 us -> 110 us
    pallas_call x1, Pallas kernels: 127 us -> 83.2 us  [gather_all(): pl.pallas_call(gather_kernel, out_shape=(jax.ShapeDtypeStruct((seqs, sp *...]
    pallas_call x1, Pallas kernels: 36.1 us -> 27.1 us  [merge(): pl.pallas_call(merge_kernel, out_shape=jax.ShapeDtypeStruct((fs, lines, c...]
    reshape x0 -> x2, local copies, waits for them, and re-layouts: none -> 2.62 us  [the longest x1 1.44 us: merge(): out = out.reshape(fs, lines, sp, columns // sp).transpose(1, 2, 0, 3)]
where the time goes in v2:
time: 141 us
  Pallas kernels  110 us (78%)
  local copies, waits for them, and re-layouts  11.7 us (8%)
  matrix products  9.61 us (7%)
  other arithmetic  9.12 us (6%)
    pallas_call x1, Pallas kernels, gather_all(): pl.pallas_call(gather_kernel, out_shape=(jax.ShapeDtypeStruct((seqs, sp *...  83.2 us
    pallas_call x1, Pallas kernels, merge(): pl.pallas_call(merge_kernel, out_shape=jax.ShapeDtypeStruct((fs, lines, c...  27.1 us
    dot_general x2, matrix products, project(): jnp.dot(x, w_all[index].reshape(wide, 3 * each), preferred_element_type=j...  6.83 us
    select_n x3, other arithmetic, half(): return jnp.where(first, pair[0], pair[1])  2.91 us

profile of v2, /device:TPU:0, one launch (start us, length us, event | category | flops | bytes accessed | tf_op | source)
XLA Modules:
  0.0 141.1 jit_solution(1327248136490927009)
XLA Ops:
  0.0 1.2 broadcast_select_fusion.1
  1.5 1.0 broadcast_select_fusion.3
  2.7 1.2 copy.26.w_ref
  3.9 0.7 broadcast_select_fusion.o_ref
  4.8 1.0 fusion.11.tok_ref
  5.8 83.2 %gather_all.1 = (bf16[2,8,64,2048]{3,2,1,0:T(8,128)(2,1)}, bf16[2,8,256,384]{3,2,1,0:T(8,128)(2,1)}, bf16[2,512,1024]{2,1,0:T(8,128)(2,1)}) custom-call(bf16[2,64,2048]{2,1,0:T(8,128)(2,1)} %fusion.11.tok_ref, bf16[4,256,384]{2,1,0:T(8,128)(2,1)} %copy.26.w_ref, bf16[512,256]{1,0:T(8,128)(2,1)} %broadcast_select_fusion.o_ref), custom_call_target="tpu_custom_call" | custom-call | tf_op jit(solution)/shard_map/gather_all/pallas_call | solution.py:330
  89.0 2.4 %fusion.26 = (bf16[1,8,256,384]{3,2,1,0:T(8,128)(2,1)S(1)}, bf16[1,8,256,384]{3,2,1,0:T(8,128)(2,1)S(1)}) fusion(bf16[2,8,256,384]{3,2,1,0:T(8,128)(2,1)} %get-tuple-element.9), kind=kLoop, calls=%fused_computation.56 | loop fusion | bytes 6291456 | tf_op jit(solution)/shard_map/slice | solution.py:528
  91.4 0.7 copy-done.6
  92.2 2.3 %convolution_convert_fusion = bf16[1024,384]{1,0:T(8,128)(2,1)S(1)} fusion(bf16[1024,2048]{1,0:T(8,128)(2,1)S(1)} %bitcast.49, bf16[2048,384]{1,0:T(8,128)(2,1)S(1)} %bitcast.40), kind=kOutput, calls=%fused_computation.10 | convolution fusion | flops 1611005952 | bytes 6553600 | tf_op jit(solution)/shard_map/dot_general | solution.py:527
  94.7 0.9 fusion.17
  95.6 4.5 %convolution_convert_fusion.1 = bf16[1024,384]{1,0:T(8,128)(2,1)S(1)} fusion(bf16[1024,2048]{1,0:T(8,128)(2,1)} %bitcast.48, bf16[2048,384]{1,0:T(8,128)(2,1)S(1)} %bitcast.39), kind=kOutput, calls=%fused_computation.11 | convolution fusion | flops 1611005952 | bytes 6553600 | tf_op jit(solution)/shard_map/dot_general | solution.py:527
  101.1 0.8 dynamic_slice.12
  102.5 0.4 reshape.97
  103.1 0.8 dynamic_slice.13
  104.4 0.9 fusion
  105.3 0.9 fusion.1
  106.2 1.8 %fusion.12 = f32[2,2,512,128]{3,2,1,0:T(8,128)S(1)} fusion(bf16[2,512,128,1]{2,1,3,0:T(8,128)(2,1)S(1)} %bitcast.47, f32[2,2,512,512]{2,3,1,0:T(8,128)S(1)} %get-tuple-element.22, f32[2,2,512]{2,1,0:T(2,128)S(1)} %get-tuple-element.21, pred[512,512]{0,1:T(8,128)(4,1)S(1)} %iota_compare_fusion, f32[2,2,512]{2,1,0:T(2,128)S(1)} %fusion.1), kind=kOutput, calls=%fused_computation.18 | convolution fusion | flops 272891904 | bytes 5783552 | tf_op jit(solution)/shard_map/bmqk,bkd->bmqd/dot_general | solution.py:495
  108.1 0.6 dynamic_slice.14
  108.7 0.9 multiply_reduce_fusion
  109.6 0.9 multiply_convert_fusion.1.attn_ref
  110.5 27.1 %merge.1 = bf16[2,128,1024]{2,1,0:T(8,128)(2,1)} custom-call(bf16[2,4,128,128]{3,2,1,0:T(8,128)(2,1)} %multiply_convert_fusion.1.attn_ref, bf16[2,4,128,128]{3,2,1,0:T(8,128)(2,1)} %bitcast.41, bf16[2,512,1024]{2,1,0:T(8,128)(2,1)} %get-tuple-element.10.o_ref), custom_call_target="tpu_custom_call" | custom-call | tf_op jit(solution)/shard_map/merge/pallas_call | solution.py:464
  137.6 1.4 %reshape.94 = bf16[2,128,4,256]{3,2,1,0:T(4,128)(2,1)S(1)} reshape(bf16[2,128,1024]{2,1,0:T(8,128)(2,1)} %merge.1) | data formatting | bytes 1048576 | tf_op jit(solution)/shard_map/reshape | solution.py:483
  139.1 0.8 copy.32
  139.9 1.2 reshape.95
  (41 shorter events, 3.1 us)
Async XLA Ops:
  0.0 94.7 %copy-start = (f32[3,512]{1,0:T(4,128)S(1)}, f32[3,512]{1,0:T(4,128)}, u32[]{:S(2)}) copy-start(f32[3,512]{1,0:T(4,128)} %param.27) | copy-start | bytes 18436
  0.0 3.9 %copy-start.2 = (bf16[512,256]{1,0:T(8,128)(2,1)S(1)}, bf16[512,256]{1,0:T(8,128)(2,1)}, u32[]{:S(2)}) copy-start(bf16[512,256]{1,0:T(8,128)(2,1)} %param.28) | copy-start | bytes 786436
  0.0 3.9 %copy-start.3 = (bf16[512,256]{1,0:T(8,128)(2,1)S(1)}, bf16[512,256]{1,0:T(8,128)(2,1)}, u32[]{:S(2)}) copy-start(bf16[512,256]{1,0:T(8,128)(2,1)} %param.29) | copy-start | bytes 786436
  0.0 4.6 %copy-start.1 = (bf16[2,64,2048]{2,1,0:T(8,128)(2,1)S(1)}, bf16[2,64,2048]{2,1,0:T(8,128)(2,1)}, u32[]{:S(2)}) copy-start(bf16[2,64,2048]{2,1,0:T(8,128)(2,1)} %param.15) | copy-start | bytes 1572868
  0.0 4.8 %copy-start.4 = (f32[2048]{0:T(1024)S(1)}, f32[2048]{0:T(1024)}, u32[]{:S(2)}) copy-start(f32[2048]{0:T(1024)} %param.16) | copy-start | bytes 24580
  89.0 3.1 %copy-start.6 = (bf16[2,8,64,2048]{3,2,1,0:T(8,128)(2,1)S(1)}, bf16[2,8,64,2048]{3,2,1,0:T(8,128)(2,1)}, u32[]{:S(2)}) copy-start(bf16[2,8,64,2048]{3,2,1,0:T(8,128)(2,1)} %get-tuple-element.8) | copy-start | bytes 12582916
  106.2 1.9 %copy-start.7 = (f32[4]{0:T(128)S(1)}, f32[4]{0:T(128)}, u32[]{:S(2)}) copy-start(f32[4]{0:T(128)} %param.22) | copy-start | bytes 52
  106.2 3.4 %copy-start.5 = (f32[128]{0:T(128)S(1)}, f32[128]{0:T(128)}, u32[]{:S(2)}) copy-start(f32[128]{0:T(128)} %param.23) | copy-start | bytes 1540

commit v3 on v2

--- a/solution.py
+++ b/solution.py
@@ -191,9 +191,11 @@
     )
 
 
-def gather_kernel(
-    tok_ref, w_ref, o_ref, tok_all, w_all, o_all,
+def layer_kernel(
+    tok_ref, w_ref, o_ref, small_ref, out_ref, tok_all, w_all, o_all, padded, own, feats,
+    mine, theirs, got, done, landed,
     send_z, recv_z, send_c, recv_c, send_t, recv_t, send_x, recv_x, send_y, recv_y, local,
+    send_f, recv_f, send_g, recv_g, swap, last,
 ):
     sp, fs = lax.axis_size("sp"), lax.axis_size("fs")
     s, f = lax.axis_index("sp"), lax.axis_index("fs")
@@ -306,114 +308,142 @@
                     go(remote(ref, ref, send_x.at[1, d, e], recv_x.at[1, d, e], peer))
             chain(1, o_mine, o_ref, s, [])
             go(remote(o_ref, o_mine(s), send_y.at[1, s], recv_y.at[1, s], y_peer))
-    for k in range(1, sp):
-        around(1, o_mine, k, o_beyond)
     for sv in range(sp):
         arrived(recv_t.at[sv], tok_at(sv, 1 - t))
-        arrived(recv_y.at[1, sv], o_at(1 - g, sv))
     for d in range(sp):
         sv = lax.rem(s + sp - d, sp)
         for turn, gv in enumerate((g, 1 - g)):
             for e in range(fs - 1):
                 fv = lax.rem(f + fs - 1 - e, fs)
                 arrived(recv_x.at[turn, d, e], w_at(gv, sv, fv))
-    for run, copy in started:
-        run(copy.wait_send)
     for copy in keep:
         copy.wait()
-
-
-def gather_all(normed, w_half, o_half, sp, fs):
-    seqs, rows, wide = normed.shape
-    any_spec = pl.BlockSpec(memory_space=pl.ANY)
-    dma = pltpu.SemaphoreType.DMA
-    return pl.pallas_call(
-        gather_kernel,
-        out_shape=(
-            jax.ShapeDtypeStruct((seqs, sp * 2, rows, wide), jnp.bfloat16),
-            jax.ShapeDtypeStruct((2, sp * fs) + w_half.shape[1:], jnp.bfloat16),
-            jax.ShapeDtypeStruct((2, o_half.shape[0], o_half.shape[1] * sp), jnp.bfloat16),
-        ),
-        in_specs=[any_spec] * 3,
-        out_specs=[any_spec] * 3,
-        scratch_shapes=[
-            dma((sp,)), dma((sp,)), dma((2, 2, sp)), dma((2, sp)), dma((sp,)), dma((sp,)),
-            dma((2, sp, fs - 1)), dma((2, sp, fs - 1)), dma((2, sp)), dma((2, sp)), dma((3,)),
-        ],
-        compiler_params=pltpu.CompilerParams(collective_id=0, has_side_effects=True),
-        name="gather_all",
-    )(normed, w_half, o_half)
-
-
-def merge_kernel(
-    attn_ref, conv_ref, o_ref, out_ref, feats, weights, mine, theirs, got, done, landed,
-    send, recv, send_x, recv_x, swap, last, local,
-):
-    sp, fs = lax.axis_size("sp"), lax.axis_size("fs")
-    s, t, f = lax.axis_index("sp"), lax.axis_index("tp"), lax.axis_index("fs")
-    z_peers = [{"sp": lax.rem(s + d, sp)} for d in range(1, sp)]
-    x_peers = [{"fs": lax.rem(f + d, fs)} for d in range(1, fs)]
-    t_peer = {"tp": 1 - t}
-    greet(z_peers + x_peers + [t_peer])
-    seqs, unused, rows, wide = attn_ref.shape
-    half = rows // 2
-    refs = (attn_ref, conv_ref)
-    started = []
-
-    def go(copy):
-        copy.start()
-        started.append(copy)
-        return copy
-
-    for d in range(1, sp):
-        to = lax.rem(s + d, sp)
-        for kind, ref in enumerate(refs):
+    around(1, o_mine, 1, o_beyond)
+
+    seqs, shards, part, wide = tok_all.shape
+    count, each = shards * part, own.shape[4]
+    rows = count // sp
+    depth = w_all.shape[1] * w_all.shape[2]
+
+    def project(b, index):
+        out = jnp.dot(
+            tok_all[b].reshape(count, wide),
+            w_all[index].reshape(depth, 3 * each),
+            preferred_element_type=jnp.float32,
+        ).astype(jnp.bfloat16)
+        return [out[:, n * each : (n + 1) * each] for n in range(3)]
+
+    def send_feats(b):
+        for d in range(1, sp):
+            to = lax.rem(s + d, sp)
             go(
                 remote(
-                    ref.at[:, to], feats.at[f, kind, s], send.at[kind, d], recv.at[kind, d],
-                    {"sp": to},
+                    own.at[b, to], feats.at[f, s, b], send_f.at[b, d], recv_f.at[b, d], {"sp": to}
                 )
             )
-    for kind, ref in enumerate(refs):
         for e, peer in enumerate(x_peers):
             go(
                 remote(
-                    ref.at[:, s], feats.at[f, kind, s], send_x.at[kind, 0, e],
-                    recv_x.at[kind, 0, e], peer,
+                    own.at[b, s], feats.at[f, s, b], send_g.at[b, 0, e], recv_g.at[b, 0, e], peer
                 )
             )
-    fetch = pltpu.make_async_copy(o_ref, weights, local.at[2])
-    fetch.start()
-    keep = [
-        pltpu.make_async_copy(ref.at[:, s], feats.at[f, kind, s], local.at[kind])
-        for kind, ref in enumerate(refs)
-    ]
-    for copy in keep:
-        copy.start()
-    for d in range(1, sp):
-        sv = lax.rem(s + sp - d, sp)
-        for kind in range(2):
-            ref = feats.at[f, kind, sv]
-            remote(ref, ref, send.at[kind, d], recv.at[kind, d], t_peer).wait_recv()
+
+    def relay_feats(b):
+        for d in range(1, sp):
+            ref = feats.at[f, lax.rem(s + sp - d, sp), b]
+            arrived(recv_f.at[b, d], ref)
             for e, peer in enumerate(x_peers):
-                go(remote(ref, ref, send_x.at[kind, d, e], recv_x.at[kind, d, e], peer))
-    for copy in keep:
-        copy.wait()
-    fetch.wait()
+                go(remote(ref, ref, send_g.at[b, d, e], recv_g.at[b, d, e], peer))
+
+    first = lax.broadcasted_iota(jnp.int32, (count, each), 1) < DK
+
+    def pair_norm(raw, gain):
+        value = raw.astype(jnp.float32)
+        square = value * value
+        low = jnp.sum(jnp.where(first, square, 0.0), axis=-1, keepdims=True) * (1.0 / DK)
+        high = jnp.sum(jnp.where(first, 0.0, square), axis=-1, keepdims=True) * (1.0 / DK)
+        return value * jnp.where(first, lax.rsqrt(low + EPS), lax.rsqrt(high + EPS)) * gain
+
+    def attend(b):
+        query_raw, key_raw, value = project(b, 0)
+        query = pair_norm(query_raw, small_ref[0:1])
+        key = pair_norm(key_raw, small_ref[1:2]).astype(jnp.bfloat16)
+        pairs = [
+            jnp.where(first, query, 0.0).astype(jnp.bfloat16),
+            jnp.where(first, 0.0, query).astype(jnp.bfloat16),
+        ]
+        for i in range(sp):
+            seen = (i + 1) * rows
+            row = lax.broadcasted_iota(jnp.int32, (rows, seen), 0) + i * rows
+            allowed = lax.broadcasted_iota(jnp.int32, (rows, seen), 1) <= row
+            maps = []
+            for pair in pairs:
+                score = lax.dot_general(
+                    pair[i * rows : seen], key[:seen], (((1,), (1,)), ((), ())),
+                    preferred_element_type=jnp.float32,
+                ) * DK ** (-0.5)
+                score = jnp.where(allowed, score, NEG)
+                weights = jnp.exp(score - jnp.max(score, axis=-1, keepdims=True))
+                total = jnp.sum(weights, axis=-1, keepdims=True)
+                summed = jnp.dot(
+                    weights.astype(jnp.bfloat16), value[:seen], preferred_element_type=jnp.float32
+                )
+                maps.append(summed / total)
+            differ = maps[0] - small_ref[3:4] * maps[1]
+            scale = lax.rsqrt(jnp.mean(differ * differ, axis=-1, keepdims=True) + EPS)
+            own[b, i, 0] = (differ * scale * small_ref[2:3] * OUT_SCALE).astype(jnp.bfloat16)
+
+    def convolve(b):
+        gate_b, gate_c, conv_in = project(b, 1)
+        shaped = (gate_c.astype(jnp.float32) * conv_in.astype(jnp.float32)).astype(jnp.bfloat16)
+        front = padded.shape[0] - count
+        padded[0:front] = jnp.zeros((front, each), jnp.float32)
+        padded[front:] = shaped.astype(jnp.float32)
+        conv = jnp.zeros((count, each), jnp.float32)
+        for tap in range(KW):
+            begin = front - (KW - 1) + tap
+            conv = conv + small_ref[4 + tap : 5 + tap] * padded[begin : begin + count]
+        conv_out = (gate_b.astype(jnp.float32) * conv).astype(jnp.bfloat16)
+        for i in range(sp):
+            own[b, i, 1] = conv_out[i * rows : (i + 1) * rows]
+
+    o_turns = list(range(2, sp))
+    for b in range(seqs):
+        convolve(b)
+        if o_turns:
+            around(1, o_mine, o_turns.pop(0), o_beyond)
+        attend(b)
+        if o_turns:
+            around(1, o_mine, o_turns.pop(0), o_beyond)
+        send_feats(b)
+        if b:
+            relay_feats(b - 1)
+    for k in o_turns:
+        around(1, o_mine, k, o_beyond)
+    for b in range(seqs):
+        keep = pltpu.make_async_copy(own.at[b, s], feats.at[f, s, b], local.at[3 + b])
+        keep.start()
+    relay_feats(seqs - 1)
+    for b in range(seqs):
+        pltpu.make_async_copy(own.at[b, s], feats.at[f, s, b], local.at[3 + b]).wait()
+    for sv in range(sp):
+        arrived(recv_y.at[1, sv], o_at(1 - g, sv))
+    half = rows // 2
+    lines = seqs * half
 
     def product(fv, tv):
-        total = jnp.zeros((seqs * half, weights.shape[2]), jnp.float32)
+        total = jnp.zeros((lines, o_all.shape[2]), jnp.float32)
         for kind in range(2):
             left = jnp.concatenate(
                 [
-                    feats[fv, kind, sv, :, pl.ds(pl.multiple_of(tv * half, half), half), :].reshape(
-                        seqs * half, wide
-                    )
+                    feats[
+                        fv, sv, :, kind, pl.ds(pl.multiple_of(tv * half, half), half), :
+                    ].reshape(lines, each)
                     for sv in range(sp)
                 ],
                 axis=1,
             )
-            total = total + jnp.dot(left, weights[kind], preferred_element_type=jnp.float32)
+            total = total + jnp.dot(left, o_all[kind], preferred_element_type=jnp.float32)
         return total
 
     swaps, lasts = [], []
@@ -422,81 +452,70 @@
         if e:
             for d in range(sp):
                 sv = lax.rem(s + sp - d, sp)
-                for kind in range(2):
-                    ref = feats.at[fv, kind, sv]
-                    remote(
-                        ref, ref, send_x.at[kind, d, fs - 1 - e], recv_x.at[kind, d, fs - 1 - e],
-                        t_peer,
-                    ).wait_recv()
+                for b in range(seqs):
+                    arrived(recv_g.at[b, d, fs - 1 - e], feats.at[fv, sv, b])
         theirs[e] = product(fv, 1 - t).astype(jnp.bfloat16)
-        swaps.append(
-            go(remote(theirs.at[e], got.at[e], swap.at[0, e], swap.at[1, e], t_peer))
-        )
+        copy = remote(theirs.at[e], got.at[e], swap.at[0, e], swap.at[1, e], t_peer)
+        go(copy)
+        swaps.append(copy)
         mine[e] = product(fv, t)
     for e in list(range(1, fs)) + [0]:
         swaps[e].wait_recv()
         total = (mine[e] + got[e].astype(jnp.float32)).astype(jnp.bfloat16)
         if e:
             done[e - 1] = total
-            lasts.append(
-                go(
-                    remote(
-                        done.at[e - 1], landed.at[e - 1], last.at[0, e - 1], last.at[1, e - 1],
-                        x_peers[e - 1],
-                    )
-                )
-            )
+            copy = remote(
+                done.at[e - 1], landed.at[e - 1], last.at[0, e - 1], last.at[1, e - 1],
+                x_peers[e - 1],
+            )
+            go(copy)
+            lasts.append(copy)
         else:
             out_ref[f] = total
     for e in range(1, fs):
         lasts[e - 1].wait_recv()
         out_ref[lax.rem(f + fs - e, fs)] = landed[e - 1]
-    for copy in started:
-        copy.wait_send()
-
-
-def merge(attn, conv_out, o_all, fs):
-    seqs, sp, rows, wide = attn.shape
-    columns = o_all.shape[2]
-    lines = seqs * (rows // 2)
+    for run, copy in started:
+        run(copy.wait_send)
+
+
+def layer(normed, w_half, o_half, small, sp, fs):
+    seqs, part, wide = normed.shape
+    rows, each = part * 2, w_half.shape[2] // 3
+    count, lines = rows * sp, seqs * part
+    columns = o_half.shape[1] * sp
     any_spec = pl.BlockSpec(memory_space=pl.ANY)
+    vmem_spec = pl.BlockSpec(memory_space=pltpu.VMEM)
     dma = pltpu.SemaphoreType.DMA
+    narrow = functools.partial(pltpu.VMEM, dtype=jnp.bfloat16)
     out = pl.pallas_call(
-        merge_kernel,
+        layer_kernel,
         out_shape=jax.ShapeDtypeStruct((fs, lines, columns), jnp.bfloat16),
-        in_specs=[any_spec] * 3,
-        out_specs=pl.BlockSpec(memory_space=pltpu.VMEM),
+        in_specs=[any_spec] * 3 + [vmem_spec],
+        out_specs=vmem_spec,
         scratch_shapes=[
-            pltpu.VMEM((fs, 2, sp, seqs, rows, wide), jnp.bfloat16),
-            pltpu.VMEM(o_all.shape, jnp.bfloat16),
+            narrow((seqs, sp * 2, part, wide)),
+            narrow((2, sp * fs) + w_half.shape[1:]),
+            narrow((2, o_half.shape[0], columns)),
+            pltpu.VMEM((count + 8, each), jnp.float32),
+            narrow((seqs, sp, 2, rows, each)),
+            narrow((fs, sp, seqs, 2, rows, each)),
             pltpu.VMEM((fs, lines, columns), jnp.float32),
-            pltpu.VMEM((fs, lines, columns), jnp.bfloat16),
-            pltpu.VMEM((fs, lines, columns), jnp.bfloat16),
-            pltpu.VMEM((fs - 1, lines, columns), jnp.bfloat16),
-            pltpu.VMEM((fs - 1, lines, columns), jnp.bfloat16),
-            dma((2, sp)), dma((2, sp)), dma((2, sp, fs - 1)), dma((2, sp, fs - 1)),
-            dma((2, fs)), dma((2, fs - 1)), dma((3,)),
+            narrow((fs, lines, columns)),
+            narrow((fs, lines, columns)),
+            narrow((fs - 1, lines, columns)),
+            narrow((fs - 1, lines, columns)),
+            dma((sp,)), dma((sp,)), dma((2, 2, sp)), dma((2, sp)), dma((sp,)), dma((sp,)),
+            dma((2, sp, fs - 1)), dma((2, sp, fs - 1)), dma((2, sp)), dma((2, sp)),
+            dma((3 + seqs,)),
+            dma((seqs, sp)), dma((seqs, sp)), dma((seqs, sp, fs - 1)), dma((seqs, sp, fs - 1)),
+            dma((2, fs)), dma((2, fs - 1)),
         ],
-        compiler_params=pltpu.CompilerParams(collective_id=1, has_side_effects=True),
-        name="merge",
-    )(attn, conv_out, o_all)
+        compiler_params=pltpu.CompilerParams(collective_id=0, has_side_effects=True),
+        name="layer",
+    )(normed, w_half, o_half, small)
     out = out.reshape(fs, lines, sp, columns // sp).transpose(1, 2, 0, 3)
-    return out.reshape(seqs, rows // 2, fs * columns)
-
-
-def head_map(query, key, value, mix, head_gain):
-    seqs, count = value.shape[0], value.shape[1]
-    score = jnp.einsum("bqmd,bkmd->bmqk", query, key, preferred_element_type=jnp.float32)
-    score = score * DK ** (-0.5)
-    place = jnp.arange(count, dtype=jnp.int32)
-    score = jnp.where(place[None, :] <= place[:, None], score, NEG)
-    weights = jnp.exp(score - jnp.max(score, axis=-1, keepdims=True))
-    total = jnp.sum(weights, axis=-1)
-    summed = jnp.einsum(
-        "bmqk,bkd->bmqd", weights.astype(jnp.bfloat16), value, preferred_element_type=jnp.float32
-    )
-    mapped = summed / total[..., None]
-    return (rms_scale(mapped[:, 0] - mix * mapped[:, 1], head_gain) * OUT_SCALE).astype(jnp.bfloat16)
+    return out.reshape(seqs, part, fs * columns)
 
 
 def heads_on_device(
@@ -519,39 +538,21 @@
     ]
     w_half = jnp.stack(picked, axis=2).transpose(1, 0, 2, 3).reshape(sp, depth, 3 * each)
     o_half = half((w_out_attn, w_out_conv))
-    tok_all, w_all, o_all = gather_all(normed, w_half, o_half, sp, fs)
-    count = rows * sp * 2
-    x = tok_all.reshape(seqs * count, wide)
-
-    def project(index):
-        out = jnp.dot(
-            x, w_all[index].reshape(wide, 3 * each), preferred_element_type=jnp.float32
-        ).astype(jnp.bfloat16)
-        return [out[:, n * each : (n + 1) * each].reshape(seqs, count, each) for n in range(3)]
-
-    query_raw, key_raw, value = project(0)
-    gate_b, gate_c, conv_in = project(1)
 
     def mine(array, axis=0):
         return lax.dynamic_slice_in_dim(array, s * each, each, axis)
 
-    query = rms_scale(
-        query_raw.reshape(seqs, count, 2, DK), mine(query_gain).reshape(2, DK)
-    ).astype(jnp.bfloat16)
-    key = rms_scale(
-        key_raw.reshape(seqs, count, 2, DK), mine(key_gain).reshape(2, DK)
-    ).astype(jnp.bfloat16)
-    mix = lax.dynamic_slice_in_dim(mix_lambda, s, 1)[0]
-    attn = head_map(query, key, value, mix, head_gain)
-    shaped = (gate_c.astype(jnp.float32) * conv_in.astype(jnp.float32)).astype(jnp.bfloat16)
-    padded = jnp.pad(shaped, ((0, 0), (KW - 1, 0), (0, 0))).astype(jnp.float32)
-    taps = mine(conv_taps, 1)
-    conv = taps[0] * padded[:, 0:count]
-    for tap in range(1, KW):
-        conv = conv + taps[tap] * padded[:, tap : tap + count]
-    conv_out = (gate_b.astype(jnp.float32) * conv).astype(jnp.bfloat16)
-    shape = (seqs, sp, rows * 2, each)
-    return merge(attn.reshape(shape), conv_out.reshape(shape), o_all, fs)
+    mix = lax.dynamic_slice_in_dim(mix_lambda, s, 1)
+    small = jnp.concatenate(
+        [
+            mine(query_gain)[None],
+            mine(key_gain)[None],
+            head_gain[None],
+            jnp.broadcast_to(mix[:, None], (1, each)),
+            mine(conv_taps, 1),
+        ]
+    )
+    return layer(normed, w_half, o_half, small, sp, fs)
 
 
 def on_device(*arrays):

time: 141 us -> 118 us (0.84)
  matrix products: 9.61 us -> 0 us
  other arithmetic: 9.12 us -> 3.11 us
  Pallas kernels: 110 us -> 104 us
    dot_general x4 -> x0, matrix products: 9.61 us -> none  [the longest x2 6.83 us: project(): jnp.dot(x, w_all[index].reshape(wide, 3 * each), preferred_element_type=j...]
    pallas_call x2 -> x1, Pallas kernels: 110 us -> 104 us  [layer(): pl.pallas_call(layer_kernel, out_shape=jax.ShapeDtypeStruct((fs, lines, c...]
    convert_element_type x7 -> x0, other arithmetic: 2.59 us -> none  [the longest x1 0.91 us: head_map(): (rms_scale(mapped[:, 0] - mix * mapped[:, 1], head_gain) * OUT_SCALE).ast...]
    slice x2 -> x0, local copies, waits for them, and re-layouts: 2.41 us -> none  [the longest x1 2.39 us: project(): w_all[index].reshape(wide, 3 * each)]
    unnamed x16 -> x18, local copies, waits for them, and re-layouts: 0.76 us -> 3.1 us
    dynamic_slice x3 -> x1, local copies, waits for them, and re-layouts: 1.53 us -> 0.01 us  [mine(): return lax.dynamic_slice_in_dim(array, s * each, each, axis)]
    broadcast_in_dim x0 -> x2, local copies, waits for them, and re-layouts: none -> 1.43 us  [the longest x1 0.78 us: heads_on_device(): mine(key_gain)[None]]
where the time goes in v3:
time: 118 us
  Pallas kernels  104 us (88%)
  local copies, waits for them, and re-layouts  10.7 us (9%)
  other arithmetic  3.11 us (3%)
    pallas_call x1, Pallas kernels, layer(): pl.pallas_call(layer_kernel, out_shape=jax.ShapeDtypeStruct((fs, lines, c...  104 us
    unnamed x18, local copies, waits for them, and re-layouts  3.1 us

profile of v3, /device:TPU:0, one launch (start us, length us, event | category | flops | bytes accessed | tf_op | source)
XLA Modules:
  0.0 117.8 jit_solution(12947684659670515992)
XLA Ops:
  0.0 0.8 dynamic-slice_bitcast_fusion
  0.8 0.7 copy-done.8
  1.5 0.6 dynamic_slice.14
  2.0 0.6 broadcast_in_dim.23
  2.7 0.0 copy-start.7
  2.7 0.6 copy-done.7
  3.3 0.6 concatenate.3.small_ref
  3.9 1.1 broadcast_select_fusion.1
  5.0 0.1 copy.21
  5.2 0.1 copy.22
  5.3 0.8 copy-done.2
  6.1 0.1 copy-done.3
  6.2 0.1 copy.20
  6.4 0.1 pad_maximum_fusion
  6.5 1.2 copy.23.w_ref
  7.7 0.7 broadcast_select_fusion.o_ref
  8.4 0.4 copy-done.1
  8.8 0.2 fusion
  9.0 0.5 copy-done.6
  9.5 1.0 fusion.2.tok_ref
  10.5 103.8 %layer.1 = bf16[2,128,1024]{2,1,0:T(8,128)(2,1)} custom-call(bf16[2,64,2048]{2,1,0:T(8,128)(2,1)} %fusion.2.tok_ref, bf16[4,256,384]{2,1,0:T(8,128)(2,1)} %copy.23.w_ref, bf16[512,256]{1,0:T(8,128)(2,1)} %broadcast_select_fusion.o_ref, f32[7,128]{1,0:T(8,128)} %concatenate.3.small_ref), custom_call_target="tpu_custom_call" | custom-call | tf_op jit(solution)/shard_map/layer/pallas_call | solution.py:491
  114.3 1.4 %reshape.22 = bf16[2,128,4,256]{3,2,1,0:T(4,128)(2,1)S(1)} reshape(bf16[2,128,1024]{2,1,0:T(8,128)(2,1)} %layer.1) | data formatting | bytes 1048576 | tf_op jit(solution)/shard_map/reshape | solution.py:517
  115.8 0.8 copy.24
  116.6 1.2 %reshape.23 = bf16[2,64,2048]{2,1,0:T(8,128)(2,1)} reshape(bf16[128,4,2,256]{3,2,1,0:T(2,128)(2,1)S(1)} %copy.24) | data formatting | bytes 1048576 | tf_op jit(solution)/shard_map/reshape | solution.py:518
  (14 shorter events, 0.1 us)
Async XLA Ops:
  0.0 0.8 copy-start
  0.8 0.7 copy-start.8
  2.7 0.7 copy-start.7
  5.2 1.0 copy-start.2
  5.2 1.0 copy-start.3
  6.5 1.2 %copy-start.4 = (bf16[512,256]{1,0:T(8,128)(2,1)S(1)}, bf16[512,256]{1,0:T(8,128)(2,1)}, u32[]{:S(2)}) copy-start(bf16[512,256]{1,0:T(8,128)(2,1)} %param.28) | copy-start | bytes 786436
  6.5 1.2 %copy-start.5 = (bf16[512,256]{1,0:T(8,128)(2,1)S(1)}, bf16[512,256]{1,0:T(8,128)(2,1)}, u32[]{:S(2)}) copy-start(bf16[512,256]{1,0:T(8,128)(2,1)} %param.29) | copy-start | bytes 786436
  7.7 1.1 copy-start.1
  8.8 0.7 copy-start.6
